TPU v7x, 128 devices: a whole 4x4x4 slice. The times are simulated.
128 devices in a mesh: ep: 128 (over z, y, x, core).
Axes of the slice: x: 4, y: 4, z: 4, core: 2. Of those that a mesh axis runs over, the one named last changes fastest.
Arguments:
- tokens: bfloat16 [2560, 2048], P('ep'), may hold values from -6 to 6
- positions: int32 [2560], P('ep'), may hold values from 1024 to 16383
- state: float32 [2560, 8, 64, 128], P('ep'), may hold values from -1.6 to 1.6
- mix_gain: float32 [2048], replicated, may hold values from 0.1 to 1.9
- w_query: bfloat16 [2048, 512], replicated, may hold values from -0.125 to 0.125
- w_key: bfloat16 [2048, 512], replicated, may hold values from -0.125 to 0.125
- w_value: bfloat16 [2048, 1024], replicated, may hold values from -0.125 to 0.125
- ret_gain: float32 [1024], replicated, may hold values from 0.1 to 1.9
- w_out: bfloat16 [1024, 2048], P(None, 'ep'), may hold values from -0.1875 to 0.1875
- ffn_gain: float32 [2048], replicated, may hold values from 0.1 to 1.9
- routes: int32 [2560, 6], P('ep'), may hold values from 0 to 127, all different within a row; in each aligned block of 20 rows (0 to 19, 20 to 39, ...) at most 2 rows name the same one
- route_weights: float32 [2560, 6], P('ep'), may hold values from 0.1 to 1
- expert_gate: bfloat16 [128, 2048, 512], P('ep'), may hold values from -0.125 to 0.125
- expert_up: bfloat16 [128, 2048, 512], P('ep'), may hold values from -0.125 to 0.125
- expert_down: bfloat16 [128, 512, 2048], P('ep'), may hold values from -0.25 to 0.25
Outputs:
- result: bfloat16 [2560, 2048], P('ep')
- new_state: float32 [2560, 8, 64, 128], P('ep')
Inputs may be any that keep to these rules, and one draw needn't show every extreme that they name: `routes`: each row names 6 different experts; among the rows of one device no expert is named more than 2 times, a bound that some block reaches there.
All inputs are finite; a program needn't handle non-finite values.
Results may differ from a plain program's by a relative error of at most 0.017.
Values may be sent and summed in bfloat16 or wider, within the bound.
A program may use at most 128 MiB of HBM per device.

v0:
```python
import math

import jax
import jax.numpy as jnp
from jax import lax
from jax.sharding import PartitionSpec as P

EPS = 1e-06


def rms_scale(values, gain):
    wide = values.astype(jnp.float32)
    scaled = wide * lax.rsqrt(jnp.mean(wide * wide, axis=-1, keepdims=True) + EPS)
    return (scaled * gain).astype(jnp.bfloat16)


def rotate(field, spots):
    half = field.shape[-1] // 2
    freqs = jnp.exp(-math.log(10000.0) * jnp.arange(half, dtype=jnp.float32) / half)
    angle = spots.astype(jnp.float32)[:, None] * freqs[None, :]
    cosine = jnp.cos(angle)[:, None, :]
    sine = jnp.sin(angle)[:, None, :]
    first = field[..., :half]
    second = field[..., half:]
    return jnp.concatenate(
        [first * cosine - second * sine, second * cosine + first * sine], axis=-1
    )


def shards(
    tokens,
    positions,
    state,
    mix_gain,
    w_query,
    w_key,
    w_value,
    ret_gain,
    w_out,
    ffn_gain,
    routes,
    route_weights,
    expert_gate,
    expert_up,
    expert_down,
):
    seqs = tokens.shape[0]
    width = tokens.shape[1]
    heads = state.shape[1]
    head_k = state.shape[2]
    head_v = state.shape[3]
    normed_in = rms_scale(tokens, mix_gain)
    q_proj = jnp.dot(normed_in, w_query, preferred_element_type=jnp.float32).astype(jnp.bfloat16)
    k_proj = jnp.dot(normed_in, w_key, preferred_element_type=jnp.float32).astype(jnp.bfloat16)
    v_proj = jnp.dot(normed_in, w_value, preferred_element_type=jnp.float32).astype(jnp.bfloat16)
    queries = rotate(q_proj.astype(jnp.float32).reshape(seqs, heads, head_k), positions)
    key_rows = rotate(
        k_proj.astype(jnp.float32).reshape(seqs, heads, head_k), positions
    ) * head_k ** (-0.5)
    values = v_proj.astype(jnp.float32).reshape(seqs, heads, head_v)
    decays = 1.0 - jnp.exp2(-2.0 - jnp.arange(heads, dtype=jnp.float32))
    new_state = (
        decays[None, :, None, None] * state + key_rows[:, :, :, None] * values[:, :, None, :]
    )
    readout = jnp.einsum("thd,thdv->thv", queries, new_state)
    centre = jnp.mean(readout, axis=-1, keepdims=True)
    variance = jnp.mean(jnp.square(readout - centre), axis=-1, keepdims=True)
    normed = ((readout - centre) * lax.rsqrt(variance + EPS)).reshape(
        seqs, heads * head_v
    ) * ret_gain
    mixed = normed.astype(jnp.bfloat16)
    attended = jnp.dot(
        mixed, lax.all_gather(w_out, "ep", axis=1, tiled=True), preferred_element_type=jnp.float32
    ).astype(jnp.bfloat16)
    resid = (tokens.astype(jnp.float32) + attended.astype(jnp.float32)).astype(jnp.bfloat16)
    normed_mid = rms_scale(resid, ffn_gain)
    topk = routes.shape[1]
    row_count = seqs * topk
    held = expert_gate.shape[0]
    experts = held * lax.axis_size("ep")
    capacity = max(2, 2 * row_count // experts)
    chosen = routes.reshape(row_count)
    matches = (chosen[:, None] == jnp.arange(experts, dtype=jnp.int32)[None, :]).astype(jnp.int32)
    places = jnp.sum((jnp.cumsum(matches, axis=0) - matches) * matches, axis=1)
    slots = chosen * capacity + places
    dispatch = (slots[:, None] == jnp.arange(experts * capacity, dtype=jnp.int32)[None, :]).astype(
        jnp.bfloat16
    )
    repeated = jnp.repeat(normed_mid, topk, axis=0)
    outgoing = jnp.einsum("rs,rd->sd", dispatch, repeated, preferred_element_type=jnp.float32)
    outgoing = outgoing.astype(jnp.bfloat16).reshape(experts, capacity, width)
    arrivals = lax.all_to_all(outgoing, "ep", split_axis=0, concat_axis=0, tiled=True)
    senders = arrivals.shape[0] // held
    grouped = arrivals.reshape(senders, held, arrivals.shape[1], width)
    gate_part = jnp.einsum(
        "necd,edf->necf", grouped, expert_gate, preferred_element_type=jnp.float32
    )
    up_part = jnp.einsum("necd,edf->necf", grouped, expert_up, preferred_element_type=jnp.float32)
    hidden = (jax.nn.silu(gate_part) * up_part).astype(jnp.bfloat16)
    down_part = jnp.einsum(
        "necf,efd->necd", hidden, expert_down, preferred_element_type=jnp.float32
    )
    served = down_part.astype(jnp.bfloat16).reshape(arrivals.shape)
    returned = lax.all_to_all(served, "ep", split_axis=0, concat_axis=0, tiled=True)
    picked_rows = jnp.dot(
        dispatch, returned.reshape(experts * capacity, width), preferred_element_type=jnp.float32
    )
    mixture = jnp.sum(picked_rows.reshape(seqs, topk, width) * route_weights[:, :, None], axis=1)
    result = (resid.astype(jnp.float32) + mixture).astype(jnp.bfloat16)
    return (result, new_state)


def solution(mesh):
    placed = (
        P("ep", None),
        P("ep"),
        P("ep", None, None, None),
        P(),
        P(),
        P(),
        P(),
        P(),
        P(None, "ep"),
        P(),
        P("ep", None),
        P("ep", None),
        P("ep", None, None),
        P("ep", None, None),
        P("ep", None, None),
    )
    return jax.shard_map(
        shards,
        mesh=mesh,
        in_specs=placed,
        out_specs=(P("ep", None), P("ep", None, None, None)),
        check_vma=False,
    )
```

profile of v0, /device:TPU:1, one launch (start us, length us, event | category | flops | bytes accessed | tf_op | source)
XLA Modules:
  0.0 157.0 jit_solution(6465701753602487925)
XLA Ops:
  7.2 0.7 all-gather.2.cloned.1.call-update
  7.9 1.0 fusion.40
  9.0 2.1 %fusion.27 = f32[20,512]{1,0:T(8,128)S(1)} fusion(bf16[2048,512]{1,0:T(8,128)(2,1)} %param.19, bf16[20,2048]{1,0:T(8,128)(2,1)} %param.15, f32[2048]{0:T(1024)} %param.18, f32[20]{0:T(128)S(1)} %add_rsqrt_fusion.2), kind=kOutput, calls=%fused_computation.25 | convolution fusion | flops 42127360 | bytes 2228304 | tf_op jit(solution)/shard_map/dot_general | solution.py:53
  11.2 2.0 %fusion.26 = f32[20,512]{1,0:T(8,128)S(1)} fusion(bf16[2048,512]{1,0:T(8,128)(2,1)} %param.20, bf16[20,2048]{1,0:T(8,128)(2,1)S(1)} %copy-done.3, f32[2048]{0:T(1024)S(1)} %copy-done.4, f32[20]{0:T(128)S(1)} %add_rsqrt_fusion.2), kind=kOutput, calls=%fused_computation.23 | convolution fusion | flops 42127360 | bytes 2228304 | tf_op jit(solution)/shard_map/dot_general | solution.py:54
  13.3 3.0 %fusion.25 = f32[20,1024]{1,0:T(8,128)S(1)} fusion(bf16[2048,1024]{1,0:T(8,128)(2,1)} %param.21, bf16[20,2048]{1,0:T(8,128)(2,1)S(1)} %copy-done.3, f32[2048]{0:T(1024)S(1)} %copy-done.4, f32[20]{0:T(128)S(1)} %add_rsqrt_fusion.2), kind=kOutput, calls=%fused_computation.21 | convolution fusion | flops 84090880 | bytes 4366416 | tf_op jit(solution)/shard_map/dot_general | solution.py:55
  16.4 0.1 multiply_cosine_fusion
  16.6 0.1 multiply_subtract_fusion
  16.9 0.2 copy-done.2
  17.1 1.7 %multiply_add_fusion = f32[20,8,64,128]{3,2,1,0:T(8,128)S(1)} fusion(f32[20,8,64,128]{3,2,1,0:T(8,128)S(1)} %copy-done.2, f32[20,8,128]{2,1,0:T(8,128)S(1)} %slice.20, f32[20,8,64]{2,1,0:T(8,128)S(1)} %maximum_multiply_fusion, f32[8]{0:T(128)S(1)} %exponential_subtract_fusion), kind=kLoop, calls=%fused_computation | loop fusion | flops 3932160 | bytes 10608672 | tf_op jit(solution)/shard_map/add | solution.py:63
  18.8 0.8 fusion.53
  19.6 1.5 copy-done.1
  21.1 0.1 reduce_sum.57
  21.2 0.2 multiply_reduce_fusion.1
  21.4 0.1 subtract_multiply_fusion
  21.6 0.1 copy.38
  21.7 0.1 eq.50
  21.9 0.2 reduce_window_sum.11
  22.0 0.2 select_reduce_fusion
  22.2 59.1 %all-gather.2.cloned.1.call-done = bf16[1024,2048]{0,1:T(8,128)(2,1)} async-done(((bf16[1024,16]{0,1:T(8,128)(2,1)}), bf16[1024,2048]{0,1:T(8,128)(2,1)}) %all-gather.2.cloned.1.call-update) | async-done | bytes 4194320 | tf_op jit(solution)/shard_map/all_gather | solution.py:73
  81.3 3.5 %multiply_reduce_fusion = (f32[20]{0:T(128)S(1)}, f32[20,2048]{1,0:T(8,128)S(1)}) fusion(bf16[1024,2048]{0,1:T(8,128)(2,1)} %all-gather.2.cloned.1.call-done, f32[20,1024]{1,0:T(8,128)S(1)} %bitcast.74, f32[1024]{0:T(1024)S(1)} %copy-done.7, bf16[20,2048]{1,0:T(8,128)(2,1)S(1)} %copy-done.3), kind=kOutput, calls=%fused_computation.41 | convolution fusion | flops 84254704 | bytes 4526160 | tf_op jit(solution)/shard_map/dot_general | solution.py:72
  85.0 0.9 reshape.195
  86.0 1.6 %convolution_convert_fusion.1 = bf16[256,2048]{1,0:T(8,128)(2,1)S(1)} fusion(bf16[120,2048]{1,0:T(8,128)(2,1)} %reshape.195, s32[120]{0:T(128)S(1)} %multiply_add_fusion.4), kind=kOutput, calls=%fused_computation.2 | convolution fusion | flops 126384128 | bytes 1540576 | tf_op jit(solution)/shard_map/rs,rd->sd/dot_general | solution.py:90
  87.5 1.5 reshape.196
  89.1 24.7 %all_to_all.10 = bf16[128,2,2048]{2,1,0:T(2,128)(2,1)S(1)} all-to-all(bf16[128,2,2048]{2,1,0:T(2,128)(2,1)} %reshape.196), channel_id=1, replica_groups=mesh['ep'=128] {'ep'}, dimensions={0} | all-to-all | bytes 2097152 | tf_op jit(solution)/shard_map/all_to_all | solution.py:92
  113.8 1.5 fusion.10
  115.3 4.1 %convolution_convert_fusion = bf16[128,2,2048]{2,0,1:T(8,128)(2,1)} fusion(bf16[1,512,2048]{2,1,0:T(8,128)(2,1)S(1)} %copy-done, bf16[1,2048,512]{2,1,0:T(8,128)(2,1)} %param.28, bf16[128,2,2048]{2,1,0:T(2,128)(2,1)S(1)} %all_to_all.10, f32[128,1,2,512]{3,0,2,1:T(8,128)} %fusion.10), kind=kOutput, calls=%fused_computation.1 | convolution fusion | flops 1075052544 | bytes 6815744 | tf_op jit(solution)/shard_map/necf,efd->necd/dot_general | solution.py:100
  119.4 3.3 %copy.42 = bf16[128,2,2048]{2,1,0:T(2,128)(2,1)} copy(bf16[128,2,2048]{2,0,1:T(8,128)(2,1)} %convolution_convert_fusion) | data formatting | bytes 2097152 | tf_op jit(solution)/shard_map/convert_element_type | solution.py:103
  122.7 4.5 %all-to-all-start.1 = ((bf16[128,2,2048]{2,1,0:T(2,128)(2,1)}), bf16[128,2,2048]{2,1,0:T(2,128)(2,1)S(1)}, u32[]{:S(2)}, u32[]{:S(2)}) async-start(bf16[128,2,2048]{2,1,0:T(2,128)(2,1)} %copy.42), calls=%async_computation.1 | async-start | bytes 2097152 | tf_op jit(solution)/shard_map/all_to_all | solution.py:104
  127.5 19.2 %all-to-all-done.1 = bf16[128,2,2048]{2,1,0:T(2,128)(2,1)S(1)} async-done(((bf16[128,2,2048]{2,1,0:T(2,128)(2,1)}), bf16[128,2,2048]{2,1,0:T(2,128)(2,1)S(1)}, u32[]{:S(2)}, u32[]{:S(2)}) %all-to-all-start.1) | async-done | bytes 1048608 | tf_op jit(solution)/shard_map/all_to_all | solution.py:104
  146.6 1.2 reshape.212
  147.9 1.6 %fusion.9 = f32[20,2048]{1,0:T(8,128)S(1)} fusion(bf16[256,2048,1]{1,0,2:T(8,128)(2,1)} %reshape.212, f32[20,6]{0,1:T(8,128)S(1)} %copy-done.9, s32[20,6]{0,1:T(8,128)S(1)} %multiply_add_fusion.3), kind=kOutput, calls=%fused_computation.14 | convolution fusion | flops 126310400 | bytes 1213376 | tf_op jit(solution)/shard_map/dot_general | solution.py:105
  149.5 0.7 add_convert_fusion
  (43 shorter events, 1.0 us)
Async XLA Ops:
  7.2 108.2 %copy-start = (bf16[1,512,2048]{2,1,0:T(8,128)(2,1)S(1)}, bf16[1,512,2048]{2,1,0:T(8,128)(2,1)}, u32[]{:S(2)}) copy-start(bf16[1,512,2048]{2,1,0:T(8,128)(2,1)} %param.29) | copy-start | bytes 6291460
  7.2 4.0 %copy-start.3 = (bf16[20,2048]{1,0:T(8,128)(2,1)S(1)}, bf16[20,2048]{1,0:T(8,128)(2,1)}, u32[]{:S(2)}) copy-start(bf16[20,2048]{1,0:T(8,128)(2,1)} %param.15) | copy-start | bytes 245764
  7.2 4.0 %copy-start.4 = (f32[2048]{0:T(1024)S(1)}, f32[2048]{0:T(1024)}, u32[]{:S(2)}) copy-start(f32[2048]{0:T(1024)} %param.18) | copy-start | bytes 24580
  7.2 74.1 %all-gather.2.cloned.1.call-start = ((), (), s32[]{:S(2)}) async-start(), calls=%async_computation.2 | async-start | bytes 4227072 | tf_op jit(solution)/shard_map/all_gather | solution.py:73
  9.0 4.3 %copy-start.10 = (s32[20]{0:T(128)S(1)}, s32[20]{0:T(128)}, u32[]{:S(2)}) copy-start(s32[20]{0:T(128)} %param.16) | copy-start | bytes 244
  13.3 3.8 %copy-start.2 = (f32[20,8,64,128]{3,2,1,0:T(8,128)S(1)}, f32[20,8,64,128]{3,2,1,0:T(8,128)}, u32[]{:S(2)}) copy-start(f32[20,8,64,128]{3,2,1,0:T(8,128)} %param.17) | copy-start | bytes 15728644
  18.7 2.4 %copy-start.1 = (f32[20,8,64,128]{3,2,1,0:T(8,128)}, f32[20,8,64,128]{3,2,1,0:T(8,128)S(1)}, u32[]{:S(2)}) copy-start(f32[20,8,64,128]{3,2,1,0:T(8,128)S(1)} %multiply_add_fusion) | copy-start | bytes 15728644
  18.8 2.8 %copy-start.5 = (s32[20,6]{0,1:T(8,128)S(1)}, s32[20,6]{0,1:T(8,128)}, u32[]{:S(2)}) copy-start(s32[20,6]{0,1:T(8,128)} %param.25) | copy-start | bytes 1444
  18.8 62.5 %copy-start.7 = (f32[1024]{0:T(1024)S(1)}, f32[1024]{0:T(1024)}, u32[]{:S(2)}) copy-start(f32[1024]{0:T(1024)} %param.22) | copy-start | bytes 12292
  81.3 3.5 %copy-start.6 = (f32[2048]{0:T(1024)S(1)}, f32[2048]{0:T(1024)}, u32[]{:S(2)}) copy-start(f32[2048]{0:T(1024)} %param.24) | copy-start | bytes 24580
  89.1 24.8 %copy-start.8 = (bf16[1,2048,512]{2,1,0:T(8,128)(2,1)S(1)}, bf16[1,2048,512]{2,1,0:T(8,128)(2,1)}, u32[]{:S(2)}) copy-start(bf16[1,2048,512]{2,1,0:T(8,128)(2,1)} %param.27) | copy-start | bytes 6291460
  122.7 25.1 %copy-start.9 = (f32[20,6]{0,1:T(8,128)S(1)}, f32[20,6]{0,1:T(8,128)}, u32[]{:S(2)}) copy-start(f32[20,6]{0,1:T(8,128)} %param.26) | copy-start | bytes 1444
  122.7 23.9 %all-to-all-start.1 = ((bf16[128,2,2048]{2,1,0:T(2,128)(2,1)}), bf16[128,2,2048]{2,1,0:T(2,128)(2,1)S(1)}, u32[]{:S(2)}, u32[]{:S(2)}) async-start(bf16[128,2,2048]{2,1,0:T(2,128)(2,1)} %copy.42), calls=%async_computation.1 | async-start | bytes 2097152 | tf_op jit(solution)/shard_map/all_to_all | solution.py:104
Sparse Core Ops, SparseCore 0:
  11.1 70.0 all-gather.1
where the time goes:
time: 157 us
  waiting for transfers between devices  78.9 us (50%)
  blocking collectives  24.7 us (16%)
  matrix products  20.2 us (13%)
  between operations  14.3 us (9%)
  local copies, waits for them, and re-layouts  9.45 us (6%)
  other arithmetic  4.71 us (3%)
  starting transfers between devices  4.57 us (3%)
    all_gather x1, waiting for transfers between devices, shards(): lax.all_gather(w_out, 'ep', axis=1, tiled=True)  59.1 us
    all_to_all x1, blocking collectives, shards(): lax.all_to_all(outgoing, 'ep', split_axis=0, concat_axis=0, tiled=True)  24.7 us
    all_to_all x1, waiting for transfers between devices, shards(): lax.all_to_all(served, 'ep', split_axis=0, concat_axis=0, tiled=True)  19.2 us
    all_to_all x1, starting transfers between devices, shards(): lax.all_to_all(served, 'ep', split_axis=0, concat_axis=0, tiled=True)  4.53 us
    dot_general x1, matrix products, shards(): jnp.einsum('necf,efd->necd', hidden, expert_down, preferred_element_type=...  4.05 us
    dot_general x1, matrix products, shards(): jnp.dot(mixed, lax.all_gather(w_out, 'ep', axis=1, tiled=True), preferred...  3.51 us
    convert_element_type x1, local copies, waits for them, and re-layouts, shards(): served = down_part.astype(jnp.bfloat16).reshape(arrivals.shape)  3.34 us
  transfers between devices with their start and end apart: 2, of which 2 were waited for; matrix products, arithmetic and copies ran while one was open for 8% of the time, Pallas kernels for 0%

commit v1 on v0

v1 whole, which is shorter than its diff:
```python
import math

import jax
import jax.numpy as jnp
from jax import lax
from jax.experimental import pallas as pl
from jax.experimental.pallas import tpu as pltpu
from jax.sharding import PartitionSpec as P

MESH = pl.DeviceIdType.MESH
EPS = 1e-06
BF = jnp.bfloat16
F32 = jnp.float32
CUTS = ((0, 384), (384, 768), (768, 1024))
STRIDES = (32, 8, 2)
ORDERS = ((0, 1, 2), (1, 2, 0), (2, 0, 1))


def kernel(
    tokens, pos, mixg, retg, ffng, routes_t, rw_t,
    state, wq, wk, wv, wo, eg, eu, ed,
    result, new_state,
    sbuf, wqv, wkv, wvv, wh, egv, euv, edv,
    xin, tab, kt, qt, vt, rt, mix, mix_in, att, att_in, nm, dmask, chl, rsd, xs, hid,
    send1, recv1, send2, recv2,
    lsem, ssem_in, ssem_out, ag_s, ag_r, ps, pr, a_s, a_r, b_s, b_r,
):
    me = lax.axis_index("ep")
    co = (me // 32, (me // 8) % 4, (me // 2) % 4)
    c = me % 2
    chip = me // 2
    partner = me + 1 - 2 * c
    n_tok = tokens.shape[0]

    cp_wo = pltpu.make_async_copy(wo, wh.at[chip], lsem.at[0])
    cp_wo.start()
    cp_q = pltpu.make_async_copy(wq, wqv, lsem.at[1])
    cp_k = pltpu.make_async_copy(wk, wkv, lsem.at[2])
    cp_v = pltpu.make_async_copy(wv, wvv, lsem.at[3])
    cp_k.start()
    cp_q.start()
    cp_v.start()

    def state_in(h):
        return pltpu.make_async_copy(state.at[:, h], sbuf.at[h], ssem_in.at[h])

    def state_out(h):
        return pltpu.make_async_copy(sbuf.at[h], new_state.at[:, h], ssem_out.at[h])

    for h in range(8):
        state_in(h).start()
    cp_g = pltpu.make_async_copy(eg.at[0], egv, lsem.at[4])
    cp_u = pltpu.make_async_copy(eu.at[0], euv, lsem.at[5])
    cp_d = pltpu.make_async_copy(ed.at[0], edv, lsem.at[6])
    cp_g.start()
    cp_u.start()
    cp_d.start()

    def along(axis, d):
        return me + ((co[axis] + d) % 4 - co[axis]) * STRIDES[axis]

    bar = pltpu.get_barrier_semaphore()
    pl.semaphore_signal(bar, inc=1, device_id=(partner,), device_id_type=MESH)
    for axis in range(3):
        for d in (1, 2, 3):
            pl.semaphore_signal(bar, inc=1, device_id=(along(axis, d),), device_id_type=MESH)

    wide = tokens[...].astype(F32)
    scaled = wide * lax.rsqrt(jnp.mean(wide * wide, axis=-1, keepdims=True) + EPS)
    xin[...] = jnp.zeros(xin.shape, BF)
    xin[0:n_tok, :] = (scaled * mixg[...]).astype(BF)

    tab[...] = jnp.full(tab.shape, -1, jnp.int32)
    tab[0:6, 0:n_tok] = routes_t[...]
    tab[8:9, 0:n_tok] = pos[...]
    wtab = jnp.concatenate([rw_t[...], jnp.zeros((6, 128 - n_tok), F32)], axis=1)
    rows = lax.broadcasted_iota(jnp.int32, (256, 128), 0)
    expert = rows // 2
    slot = (rows % 2).astype(F32)
    member = jnp.zeros((256, 128), F32)
    weight = jnp.zeros((256, 128), F32)
    for k in range(6):
        hit = tab[k : k + 1, :] == expert
        member = member + jnp.where(hit, 1.0, 0.0)
        weight = weight + jnp.where(hit, wtab[k : k + 1, :], 0.0)
    before = jnp.where(
        lax.broadcasted_iota(jnp.int32, (128, 128), 0) < lax.broadcasted_iota(jnp.int32, (128, 128), 1), 1.0, 0.0
    ).astype(BF)
    place = jnp.dot(member.astype(BF), before, preferred_element_type=F32)
    chosen = jnp.where(place == slot, member, 0.0)
    dmask[...] = chosen.astype(BF)
    comb = (chosen * weight).T
    high = comb.astype(BF)
    chl[0:32, :] = high[0:32, :]
    chl[32:64, :] = (comb - high.astype(F32)).astype(BF)[0:32, :]

    spots = tab[8:9, 0:32].astype(F32)
    freqs = jnp.exp(-math.log(10000.0) * lax.broadcasted_iota(jnp.int32, (32, 32), 0).astype(F32) / 32.0)
    angle = spots * freqs
    cosine = jnp.cos(angle)
    sine = jnp.sin(angle)

    def send_block(cc, j, phase):
        axis = ORDERS[j][phase]
        where = (cc[0] * 4 + cc[1]) * 4 + cc[2]
        piece = wh.at[where, :, pl.ds(CUTS[j][0], CUTS[j][1] - CUTS[j][0])]
        for d in (1, 3, 2):
            pltpu.make_async_remote_copy(
                src_ref=piece, dst_ref=piece, send_sem=ag_s, recv_sem=ag_r.at[phase, j],
                device_id=(along(axis, d),), device_id_type=MESH,
            ).start()

    def wait_phase(phase, j):
        n = 3 * 4**phase
        seen = wh.at[pl.ds(0, n), :, pl.ds(CUTS[j][0], CUTS[j][1] - CUTS[j][0])]
        pltpu.make_async_copy(seen, seen, ag_r.at[phase, j]).wait()

    pl.semaphore_wait(bar, 10)
    cp_wo.wait()
    for j in range(3):
        for phase in range(3):
            send_block(co, j, phase)

    def project(wref, n):
        return jnp.dot(xin[...], wref[:, n * 256 : (n + 1) * 256], preferred_element_type=F32).astype(BF).astype(F32)

    def rotated(dst, wref, scale):
        for n in range(2):
            cols = project(wref, n).T
            for s in range(4):
                a = cols[s * 64 : s * 64 + 32, :]
                b = cols[s * 64 + 32 : s * 64 + 64, :]
                dst[n * 4 + s, 0:32, :] = (a * cosine - b * sine) * scale
                dst[n * 4 + s, 32:64, :] = (b * cosine + a * sine) * scale

    cp_k.wait()
    rotated(kt, wkv, 0.125)
    cp_q.wait()
    rotated(qt, wqv, 1.0)

    def forward0():
        for j in range(3):
            wait_phase(0, j)
            a0 = ORDERS[j][0]

            def step(d, _):
                cc = list(co)
                cc[a0] = (co[a0] + d) % 4
                send_block(cc, j, 1)
                send_block(cc, j, 2)
                return 0

            lax.fori_loop(1, 4, step, 0)

    def forward1():
        for j in range(3):
            wait_phase(1, j)
            a0, a1 = ORDERS[j][0], ORDERS[j][1]

            def step(i, _):
                cc = list(co)
                cc[a0] = (co[a0] + i % 4) % 4
                cc[a1] = (co[a1] + 1 + i // 4) % 4
                send_block(cc, j, 2)
                return 0

            lax.fori_loop(0, 12, step, 0)

    forward0()
    cp_v.wait()
    for n in range(4):
        part = project(wvv, n)
        vt[2 * n] = part[:, 0:128]
        vt[2 * n + 1] = part[:, 128:256]

    def head(h, power):
        state_in(h).wait()
        decay = 1.0 - power
        for t in range(n_tok):
            new = decay * sbuf[h, t] + kt[h, :, t : t + 1] * vt[h, t : t + 1, :]
            sbuf[h, t] = new
            rt[h, t : t + 1, :] = jnp.sum(qt[h, :, t : t + 1] * new, axis=0, keepdims=True)
        state_out(h).start()
        return power * 0.5

    power = lax.fori_loop(0, 3, head, jnp.float32(0.25))
    forward1()
    lax.fori_loop(3, 8, head, power)

    for h in range(8):
        read = rt[h, 0:n_tok, :]
        centred = read - jnp.mean(read, axis=-1, keepdims=True)
        normed = centred * lax.rsqrt(jnp.mean(centred * centred, axis=-1, keepdims=True) + EPS)
        mix[0:n_tok, h * 128 : (h + 1) * 128] = (normed * retg[:, h * 128 : (h + 1) * 128]).astype(BF)

    to_partner = pltpu.make_async_remote_copy(
        src_ref=mix, dst_ref=mix_in, send_sem=ps.at[0], recv_sem=pr.at[0], device_id=(partner,), device_id_type=MESH
    )
    to_partner.start()
    nm[...] = jnp.zeros(nm.shape, BF)

    srow = lax.broadcasted_iota(jnp.int32, (256, 256), 0)
    scol = lax.broadcasted_iota(jnp.int32, (256, 256), 1)
    owner = jnp.where(srow < 128, c, 1 - c)
    target = ((srow % 128) // 16) * 32 + owner * 16 + srow % 16
    spread = jnp.where(scol == target, 1.0, 0.0).astype(BF)

    to_partner.wait()
    for j in range(3):
        wait_phase(2, j)
    both = jnp.concatenate([mix[...], mix_in[...]], axis=0)
    for n in range(4):
        block = wh[n * 16 : (n + 1) * 16].reshape(256, 1024)
        att[:, n * 256 : (n + 1) * 256] = lax.dot_general(
            both, block, (((1,), (1,)), ((), ())), preferred_element_type=F32
        ).astype(BF)
    swap = pltpu.make_async_remote_copy(
        src_ref=att.at[pl.ds(32, 32)], dst_ref=att_in, send_sem=ps.at[1], recv_sem=pr.at[1],
        device_id=(partner,), device_id_type=MESH,
    )
    swap.start()
    swap.wait()
    total = jnp.zeros((n_tok, 1), F32)
    for n in range(8):
        halves = jnp.concatenate([att[0:32, n * 128 : (n + 1) * 128], att_in[:, n * 128 : (n + 1) * 128]], axis=1)
        attended = jnp.dot(halves, spread, preferred_element_type=F32)
        cols = slice(n * 256, (n + 1) * 256)
        res = (tokens[:, cols].astype(F32) + attended[0:n_tok, :]).astype(BF).astype(F32)
        rsd[:, cols] = res
        total = total + jnp.sum(res * res, axis=-1, keepdims=True)
    inv = lax.rsqrt(total / 2048.0 + EPS)
    nm[0:n_tok, :] = (rsd[...] * inv * ffng[...]).astype(BF)

    for n in range(8):
        cols = slice(n * 256, (n + 1) * 256)
        out = jnp.dot(dmask[:, 0:32], nm[:, cols], preferred_element_type=F32).astype(BF)
        send1[:, :, cols] = out.reshape(128, 2, 256)

    def exchange(src, dst, ss, rs):
        def body(i, _):
            j = (i * 37) % 128
            t = ((co[0] + j // 32) % 4) * 32 + ((co[1] + (j // 8) % 4) % 4) * 8 + ((co[2] + (j // 2) % 4) % 4) * 2 + (c + j) % 2
            pltpu.make_async_remote_copy(
                src_ref=src.at[t], dst_ref=dst.at[me], send_sem=ss, recv_sem=rs, device_id=(t,), device_id_type=MESH
            ).start()
            return 0

        lax.fori_loop(1, 128, body, 0)
        dst[me] = src[me]

    def finish(src, dst, ss, rs):
        a = dst.at[pl.ds(0, 127)]
        pltpu.make_async_copy(a, a, rs).wait()
        b = src.at[pl.ds(0, 127)]
        pltpu.make_async_copy(b, b, ss).wait()

    exchange(send1, recv1, a_s, a_r)
    cp_g.wait()
    cp_u.wait()
    cp_d.wait()
    finish(send1, recv1, a_s, a_r)

    def unpack(i, _):
        xs[pl.ds(i * 16, 16), :] = recv1[pl.ds(i * 8, 8)].reshape(16, 2048)
        return 0

    lax.fori_loop(0, 16, unpack, 0)
    for n in range(2):
        cols = slice(n * 256, (n + 1) * 256)
        gate = jnp.dot(xs[...], egv[:, cols], preferred_element_type=F32)
        up = jnp.dot(xs[...], euv[:, cols], preferred_element_type=F32)
        hid[:, cols] = (jax.nn.silu(gate) * up).astype(BF)
    for n in range(8):
        cols = slice(n * 256, (n + 1) * 256)
        out = jnp.dot(hid[...], edv[:, cols], preferred_element_type=F32).astype(BF)
        send2[:, :, cols] = out.reshape(128, 2, 256)

    exchange(send2, recv2, b_s, b_r)
    finish(send2, recv2, b_s, b_r)

    def unpack2(i, _):
        xs[pl.ds(i * 16, 16), :] = recv2[pl.ds(i * 8, 8)].reshape(16, 2048)
        return 0

    lax.fori_loop(0, 16, unpack2, 0)
    for n in range(8):
        cols = slice(n * 256, (n + 1) * 256)
        got = jnp.dot(chl[...], xs[:, cols], preferred_element_type=F32)
        result[:, cols] = (rsd[:, cols] + got[0:n_tok, :] + got[32 : 32 + n_tok, :]).astype(BF)

    sent = wh.at[pl.ds(0, 63)]
    pltpu.make_async_copy(sent, sent, ag_s).wait()

    def drain(h, _):
        state_out(h).wait()
        return 0

    lax.fori_loop(0, 8, drain, 0)


def shards(
    tokens, positions, state, mix_gain, w_query, w_key, w_value, ret_gain, w_out, ffn_gain,
    routes, route_weights, expert_gate, expert_up, expert_down,
):
    vmem = pl.BlockSpec(memory_space=pltpu.VMEM)
    hbm = pl.BlockSpec(memory_space=pl.ANY)
    n_tok = tokens.shape[0]
    dma = pltpu.SemaphoreType.DMA
    vm = pltpu.VMEM
    return pl.pallas_call(
        kernel,
        out_shape=(
            jax.ShapeDtypeStruct(tokens.shape, BF),
            jax.ShapeDtypeStruct(state.shape, F32),
        ),
        in_specs=[vmem] * 7 + [hbm] * 8,
        out_specs=(vmem, hbm),
        scratch_shapes=[
            vm((8, n_tok, 64, 128), F32), vm((2048, 512), BF), vm((2048, 512), BF), vm((2048, 1024), BF),
            vm((64, 16, 1024), BF), vm((2048, 512), BF), vm((2048, 512), BF), vm((512, 2048), BF),
            vm((32, 2048), BF), vm((16, 128), jnp.int32), vm((8, 64, 32), F32), vm((8, 64, 32), F32),
            vm((8, 32, 128), F32), vm((8, 32, 128), F32), vm((32, 1024), BF), vm((32, 1024), BF),
            vm((64, 1024), BF), vm((32, 1024), BF), vm((32, 2048), BF), vm((256, 128), BF), vm((64, 256), BF),
            vm((n_tok, 2048), F32), vm((256, 2048), BF), vm((256, 512), BF),
            vm((128, 2, 2048), BF), vm((128, 2, 2048), BF), vm((128, 2, 2048), BF), vm((128, 2, 2048), BF),
            dma((7,)), dma((8,)), dma((8,)), dma, dma((3, 3)), dma((2,)), dma((2,)), dma, dma, dma, dma,
        ],
        compiler_params=pltpu.CompilerParams(collective_id=0, has_side_effects=True, vmem_limit_bytes=56 << 20),
        name="layer",
    )(
        tokens, positions.reshape(1, n_tok), mix_gain.reshape(1, -1), ret_gain.reshape(1, -1), ffn_gain.reshape(1, -1),
        routes.T, route_weights.T, state, w_query, w_key, w_value, w_out.T, expert_gate, expert_up, expert_down,
    )


def solution(mesh):
    placed = (
        P("ep", None), P("ep"), P("ep", None, None, None), P(), P(), P(), P(), P(), P(None, "ep"), P(),
        P("ep", None), P("ep", None), P("ep", None, None), P("ep", None, None), P("ep", None, None),
    )
    return jax.shard_map(
        shards, mesh=mesh, in_specs=placed, out_specs=(P("ep", None), P("ep", None, None, None)), check_vma=False
    )
```

time: 157 us -> 69.6 us (0.44)
  waiting for transfers between devices: 78.9 us -> 0 us
  Pallas kernels: 0 us -> 61.5 us
  blocking collectives: 24.7 us -> 0 us
  matrix products: 20.2 us -> 0 us
  between operations: 14.3 us -> 0.64 us
  other arithmetic: 4.71 us -> 0 us
  starting transfers between devices: 4.57 us -> 0 us
  local copies, waits for them, and re-layouts: 9.45 us -> 7.24 us
    pallas_call x0 -> x1, Pallas kernels: none -> 61.5 us  [shards(): pl.pallas_call(kernel, out_shape=(jax.ShapeDtypeStruct(tokens.shape, BF),...]
    all_gather x1 -> x0, waiting for transfers between devices: 59.1 us -> none  [shards(): lax.all_gather(w_out, 'ep', axis=1, tiled=True)]
    all_to_all x1 -> x0, blocking collectives: 24.7 us -> none  [shards(): lax.all_to_all(outgoing, 'ep', split_axis=0, concat_axis=0, tiled=True)]
    dot_general x9 -> x0, matrix products: 20.2 us -> none  [the longest x1 4.05 us: shards(): jnp.einsum('necf,efd->necd', hidden, expert_down, preferred_element_type=...]
    all_to_all x1 -> x0, waiting for transfers between devices: 19.2 us -> none  [shards(): lax.all_to_all(served, 'ep', split_axis=0, concat_axis=0, tiled=True)]
    unnamed x26 -> x2, local copies, waits for them, and re-layouts: 1.93 us -> 7.24 us
    all_to_all x1 -> x0, starting transfers between devices: 4.53 us -> none  [shards(): lax.all_to_all(served, 'ep', split_axis=0, concat_axis=0, tiled=True)]
    reshape x5 -> x0, local copies, waits for them, and re-layouts: 3.84 us -> none  [the longest x1 1.52 us: shards(): outgoing = outgoing.astype(jnp.bfloat16).reshape(experts, capacity, width)]
  transfers between devices with their start and end apart: 2 -> 0, of which waited for: 2 -> 0; matrix products, arithmetic and copies ran while one was open for 8% -> 0% of each run, Pallas kernels for 0% -> 0%
where the time goes in v1:
time: 69.6 us; the launch traced here: 69.4 us
  Pallas kernels  61.5 us (88%)
  local copies, waits for them, and re-layouts  7.24 us (10%)
    pallas_call x1, Pallas kernels, shards(): pl.pallas_call(kernel, out_shape=(jax.ShapeDtypeStruct(tokens.shape, BF),...  61.5 us
    unnamed x2, local copies, waits for them, and re-layouts  7.24 us

profile of v1, /device:TPU:1, one launch (start us, length us, event | category | flops | bytes accessed | tf_op | source)
XLA Modules:
  0.0 69.4 jit_solution(4606406029061791088)
XLA Ops:
  0.6 61.5 %layer.1 = (bf16[20,2048]{1,0:T(8,128)(2,1)}, f32[20,8,64,128]{3,2,1,0:T(8,128)}) custom-call(bf16[20,2048]{1,0:T(8,128)(2,1)} %tokens.1, s32[1,20]{1,0:T(1,128)} %bitcast.13, f32[1,2048]{1,0:T(1,128)} %bitcast.8, f32[1,1024]{1,0:T(1,128)} %bitcast.10, f32[1,2048]{1,0:T(1,128)} %bitcast.9, s32[6,20]{1,0:T(8,128)} %bitcast.11, f32[6,20]{1,0:T(8,128)} %bitcast.12, ...), custom_call_target="tpu_custom_call" | custom-call | tf_op jit(solution)/shard_map/layer/pallas_call | solution.py:310
  62.1 1.5 %copy.19 = bf16[20,2048]{1,0:T(8,128)(2,1)} copy(bf16[20,2048]{1,0:T(8,128)(2,1)} %get-tuple-element.4) | data formatting | bytes 163840
  63.7 5.7 %copy.20 = f32[20,8,64,128]{3,2,1,0:T(8,128)} copy(f32[20,8,64,128]{3,2,1,0:T(8,128)} %get-tuple-element.5) | data formatting | bytes 10485760

commit v2 on v1

--- a/solution.py
+++ b/solution.py
@@ -17,13 +17,13 @@
 
 
 def kernel(
-    tokens, pos, mixg, retg, ffng, routes_t, rw_t,
+    tokens_h, pos_h, mixg_h, retg_h, ffng_h, routes_h, rw_h,
     state, wq, wk, wv, wo, eg, eu, ed,
     result, new_state,
-    sbuf, wqv, wkv, wvv, wh, egv, euv, edv,
+    tokens, pos, mixg, retg, ffng, routes_t, rw_t, wqv, wkv, wvv, wh, egv, euv, edv,
     xin, tab, kt, qt, vt, rt, mix, mix_in, att, att_in, nm, dmask, chl, rsd, xs, hid,
     send1, recv1, send2, recv2,
-    lsem, ssem_in, ssem_out, ag_s, ag_r, ps, pr, a_s, a_r, b_s, b_r,
+    lsem, ssem_in, ag_s, ag_r, ps, pr, a_s, a_r, b_s, b_r,
 ):
     me = lax.axis_index("ep")
     co = (me // 32, (me // 8) % 4, (me // 2) % 4)
@@ -32,30 +32,6 @@
     partner = me + 1 - 2 * c
     n_tok = tokens.shape[0]
 
-    cp_wo = pltpu.make_async_copy(wo, wh.at[chip], lsem.at[0])
-    cp_wo.start()
-    cp_q = pltpu.make_async_copy(wq, wqv, lsem.at[1])
-    cp_k = pltpu.make_async_copy(wk, wkv, lsem.at[2])
-    cp_v = pltpu.make_async_copy(wv, wvv, lsem.at[3])
-    cp_k.start()
-    cp_q.start()
-    cp_v.start()
-
-    def state_in(h):
-        return pltpu.make_async_copy(state.at[:, h], sbuf.at[h], ssem_in.at[h])
-
-    def state_out(h):
-        return pltpu.make_async_copy(sbuf.at[h], new_state.at[:, h], ssem_out.at[h])
-
-    for h in range(8):
-        state_in(h).start()
-    cp_g = pltpu.make_async_copy(eg.at[0], egv, lsem.at[4])
-    cp_u = pltpu.make_async_copy(eu.at[0], euv, lsem.at[5])
-    cp_d = pltpu.make_async_copy(ed.at[0], edv, lsem.at[6])
-    cp_g.start()
-    cp_u.start()
-    cp_d.start()
-
     def along(axis, d):
         return me + ((co[axis] + d) % 4 - co[axis]) * STRIDES[axis]
 
@@ -65,10 +41,34 @@
         for d in (1, 2, 3):
             pl.semaphore_signal(bar, inc=1, device_id=(along(axis, d),), device_id_type=MESH)
 
-    wide = tokens[...].astype(F32)
-    scaled = wide * lax.rsqrt(jnp.mean(wide * wide, axis=-1, keepdims=True) + EPS)
-    xin[...] = jnp.zeros(xin.shape, BF)
-    xin[0:n_tok, :] = (scaled * mixg[...]).astype(BF)
+    def fetch(n, src, dst):
+        cp = pltpu.make_async_copy(src, dst, lsem.at[n])
+        cp.start()
+        return cp
+
+    cp_tok = fetch(7, tokens_h, tokens)
+    cp_mixg = fetch(8, mixg_h, mixg)
+    cp_rt = fetch(9, routes_h, routes_t)
+    cp_rw = fetch(10, rw_h, rw_t)
+    cp_pos = fetch(11, pos_h, pos)
+    cp_wo = fetch(0, wo, wh.at[chip])
+    cp_k = fetch(1, wk, wkv)
+    cp_q = fetch(2, wq, wqv)
+    cp_v = fetch(3, wv, wvv)
+
+    def state_in(h):
+        return pltpu.make_async_copy(state.at[:, h], new_state.at[:, h], ssem_in.at[h])
+
+    for h in range(8):
+        state_in(h).start()
+    cp_retg = fetch(12, retg_h, retg)
+    cp_ffng = fetch(13, ffng_h, ffng)
+    cp_g = fetch(4, eg.at[0], egv)
+    cp_u = fetch(5, eu.at[0], euv)
+    cp_d = fetch(6, ed.at[0], edv)
+    cp_rt.wait()
+    cp_rw.wait()
+    cp_pos.wait()
 
     tab[...] = jnp.full(tab.shape, -1, jnp.int32)
     tab[0:6, 0:n_tok] = routes_t[...]
@@ -100,6 +100,13 @@
     cosine = jnp.cos(angle)
     sine = jnp.sin(angle)
 
+    cp_tok.wait()
+    cp_mixg.wait()
+    wide = tokens[...].astype(F32)
+    scaled = wide * lax.rsqrt(jnp.mean(wide * wide, axis=-1, keepdims=True) + EPS)
+    xin[...] = jnp.zeros(xin.shape, BF)
+    xin[0:n_tok, :] = (scaled * mixg[...]).astype(BF)
+
     def send_block(cc, j, phase):
         axis = ORDERS[j][phase]
         where = (cc[0] * 4 + cc[1]) * 4 + cc[2]
@@ -177,16 +184,16 @@
         state_in(h).wait()
         decay = 1.0 - power
         for t in range(n_tok):
-            new = decay * sbuf[h, t] + kt[h, :, t : t + 1] * vt[h, t : t + 1, :]
-            sbuf[h, t] = new
+            new = decay * new_state[t, h] + kt[h, :, t : t + 1] * vt[h, t : t + 1, :]
+            new_state[t, h] = new
             rt[h, t : t + 1, :] = jnp.sum(qt[h, :, t : t + 1] * new, axis=0, keepdims=True)
-        state_out(h).start()
         return power * 0.5
 
     power = lax.fori_loop(0, 3, head, jnp.float32(0.25))
     forward1()
     lax.fori_loop(3, 8, head, power)
 
+    cp_retg.wait()
     for h in range(8):
         read = rt[h, 0:n_tok, :]
         centred = read - jnp.mean(read, axis=-1, keepdims=True)
@@ -220,6 +227,7 @@
     )
     swap.start()
     swap.wait()
+    cp_ffng.wait()
     total = jnp.zeros((n_tok, 1), F32)
     for n in range(8):
         halves = jnp.concatenate([att[0:32, n * 128 : (n + 1) * 128], att_in[:, n * 128 : (n + 1) * 128]], axis=1)
@@ -236,47 +244,72 @@
         out = jnp.dot(dmask[:, 0:32], nm[:, cols], preferred_element_type=F32).astype(BF)
         send1[:, :, cols] = out.reshape(128, 2, 256)
 
-    def exchange(src, dst, ss, rs):
-        def body(i, _):
-            j = (i * 37) % 128
-            t = ((co[0] + j // 32) % 4) * 32 + ((co[1] + (j // 8) % 4) % 4) * 8 + ((co[2] + (j // 2) % 4) % 4) * 2 + (c + j) % 2
+    def peers(half, sign, put):
+        zs = [((co[0] + sign * (half + 2 * i)) % 4) * 32 for i in range(2)]
+        xs8 = [((co[2] + sign * dx) % 4) * 2 + (c + dc) % 2 for dx in range(4) for dc in range(2)]
+
+        def row(i, skip):
+            zz = jnp.where(i // 4 == 0, zs[0], zs[1])
+            base = zz + ((co[1] + sign * (i % 4) + 4) % 4) * 8
+            for n in range(8):
+                if n >= skip:
+                    put(half * 64 + i * 8 + n, base + xs8[n])
+
+        if half == 0:
+            row(jnp.int32(0), 1)
+        lax.fori_loop(1 - half, 8, lambda i, _: (row(i, 0), 0)[1], 0)
+
+    def dispatch(half):
+        def put(j, t):
             pltpu.make_async_remote_copy(
-                src_ref=src.at[t], dst_ref=dst.at[me], send_sem=ss, recv_sem=rs, device_id=(t,), device_id_type=MESH
+                src_ref=send1.at[t], dst_ref=recv1.at[j], send_sem=a_s, recv_sem=a_r.at[half],
+                device_id=(t,), device_id_type=MESH,
             ).start()
-            return 0
-
-        lax.fori_loop(1, 128, body, 0)
-        dst[me] = src[me]
-
-    def finish(src, dst, ss, rs):
-        a = dst.at[pl.ds(0, 127)]
-        pltpu.make_async_copy(a, a, rs).wait()
-        b = src.at[pl.ds(0, 127)]
-        pltpu.make_async_copy(b, b, ss).wait()
-
-    exchange(send1, recv1, a_s, a_r)
+
+        peers(half, 1, put)
+
+    def give_back(half):
+        def put(j, t):
+            pltpu.make_async_remote_copy(
+                src_ref=send2.at[j], dst_ref=recv2.at[me], send_sem=b_s, recv_sem=b_r,
+                device_id=(t,), device_id_type=MESH,
+            ).start()
+
+        peers(half, -1, put)
+
+    def arrived(buf, first, count, sem):
+        seen = buf.at[pl.ds(first, count)]
+        pltpu.make_async_copy(seen, seen, sem).wait()
+
+    def experts(half):
+        base = half * 128
+        for i in range(8):
+            xs[base + i * 16 : base + (i + 1) * 16, :] = recv1[half * 64 + i * 8 : half * 64 + (i + 1) * 8].reshape(16, 2048)
+        mine = slice(base, base + 128)
+        for n in range(2):
+            cols = slice(n * 256, (n + 1) * 256)
+            gate = jnp.dot(xs[mine, :], egv[:, cols], preferred_element_type=F32)
+            up = jnp.dot(xs[mine, :], euv[:, cols], preferred_element_type=F32)
+            hid[mine, cols] = (jax.nn.silu(gate) * up).astype(BF)
+        for n in range(8):
+            cols = slice(n * 256, (n + 1) * 256)
+            out = jnp.dot(hid[mine, :], edv[:, cols], preferred_element_type=F32).astype(BF)
+            send2[half * 64 : half * 64 + 64, :, cols] = out.reshape(64, 2, 256)
+
+    dispatch(0)
+    dispatch(1)
+    recv1[0] = send1[me]
     cp_g.wait()
     cp_u.wait()
     cp_d.wait()
-    finish(send1, recv1, a_s, a_r)
-
-    def unpack(i, _):
-        xs[pl.ds(i * 16, 16), :] = recv1[pl.ds(i * 8, 8)].reshape(16, 2048)
-        return 0
-
-    lax.fori_loop(0, 16, unpack, 0)
-    for n in range(2):
-        cols = slice(n * 256, (n + 1) * 256)
-        gate = jnp.dot(xs[...], egv[:, cols], preferred_element_type=F32)
-        up = jnp.dot(xs[...], euv[:, cols], preferred_element_type=F32)
-        hid[:, cols] = (jax.nn.silu(gate) * up).astype(BF)
-    for n in range(8):
-        cols = slice(n * 256, (n + 1) * 256)
-        out = jnp.dot(hid[...], edv[:, cols], preferred_element_type=F32).astype(BF)
-        send2[:, :, cols] = out.reshape(128, 2, 256)
-
-    exchange(send2, recv2, b_s, b_r)
-    finish(send2, recv2, b_s, b_r)
+    arrived(recv1, 1, 63, a_r.at[0])
+    experts(0)
+    give_back(0)
+    recv2[me] = send2[0]
+    arrived(recv1, 64, 64, a_r.at[1])
+    experts(1)
+    give_back(1)
+    arrived(recv2, 0, 127, b_r)
 
     def unpack2(i, _):
         xs[pl.ds(i * 16, 16), :] = recv2[pl.ds(i * 8, 8)].reshape(16, 2048)
@@ -288,14 +321,10 @@
         got = jnp.dot(chl[...], xs[:, cols], preferred_element_type=F32)
         result[:, cols] = (rsd[:, cols] + got[0:n_tok, :] + got[32 : 32 + n_tok, :]).astype(BF)
 
+    arrived(send1, 0, 127, a_s)
+    arrived(send2, 0, 127, b_s)
     sent = wh.at[pl.ds(0, 63)]
     pltpu.make_async_copy(sent, sent, ag_s).wait()
-
-    def drain(h, _):
-        state_out(h).wait()
-        return 0
-
-    lax.fori_loop(0, 8, drain, 0)
 
 
 def shards(
@@ -311,21 +340,23 @@
         kernel,
         out_shape=(
             jax.ShapeDtypeStruct(tokens.shape, BF),
-            jax.ShapeDtypeStruct(state.shape, F32),
+            pltpu.VMEM(state.shape, F32),
         ),
-        in_specs=[vmem] * 7 + [hbm] * 8,
-        out_specs=(vmem, hbm),
+        in_specs=[hbm] * 15,
+        out_specs=(vmem, vmem),
         scratch_shapes=[
-            vm((8, n_tok, 64, 128), F32), vm((2048, 512), BF), vm((2048, 512), BF), vm((2048, 1024), BF),
+            vm((n_tok, 2048), BF), vm((1, n_tok), jnp.int32), vm((1, 2048), F32), vm((1, 1024), F32), vm((1, 2048), F32),
+            vm((6, n_tok), jnp.int32), vm((6, n_tok), F32),
+            vm((2048, 512), BF), vm((2048, 512), BF), vm((2048, 1024), BF),
             vm((64, 16, 1024), BF), vm((2048, 512), BF), vm((2048, 512), BF), vm((512, 2048), BF),
             vm((32, 2048), BF), vm((16, 128), jnp.int32), vm((8, 64, 32), F32), vm((8, 64, 32), F32),
             vm((8, 32, 128), F32), vm((8, 32, 128), F32), vm((32, 1024), BF), vm((32, 1024), BF),
             vm((64, 1024), BF), vm((32, 1024), BF), vm((32, 2048), BF), vm((256, 128), BF), vm((64, 256), BF),
             vm((n_tok, 2048), F32), vm((256, 2048), BF), vm((256, 512), BF),
             vm((128, 2, 2048), BF), vm((128, 2, 2048), BF), vm((128, 2, 2048), BF), vm((128, 2, 2048), BF),
-            dma((7,)), dma((8,)), dma((8,)), dma, dma((3, 3)), dma((2,)), dma((2,)), dma, dma, dma, dma,
+            dma((14,)), dma((8,)), dma, dma((3, 3)), dma((2,)), dma((2,)), dma, dma((2,)), dma, dma,
         ],
-        compiler_params=pltpu.CompilerParams(collective_id=0, has_side_effects=True, vmem_limit_bytes=56 << 20),
+        compiler_params=pltpu.CompilerParams(collective_id=0, has_side_effects=True, vmem_limit_bytes=61718528),
         name="layer",
     )(
         tokens, positions.reshape(1, n_tok), mix_gain.reshape(1, -1), ret_gain.reshape(1, -1), ffn_gain.reshape(1, -1),

time: 69.6 us -> 61.5 us (0.88)
  local copies, waits for them, and re-layouts: 7.24 us -> 3.01 us
  Pallas kernels: 61.5 us -> 57.8 us
    unnamed x2 -> x4, local copies, waits for them, and re-layouts: 7.24 us -> 3.01 us
    pallas_call x1, Pallas kernels: 61.5 us -> 57.8 us  [shards(): pl.pallas_call(kernel, out_shape=(jax.ShapeDtypeStruct(tokens.shape, BF),...]
where the time goes in v2:
time: 61.5 us; the launch traced here: 61.4 us
  Pallas kernels  57.8 us (94%)
  local copies, waits for them, and re-layouts  3.01 us (5%)
  between operations  0.65 us (1%)
    pallas_call x1, Pallas kernels, shards(): pl.pallas_call(kernel, out_shape=(jax.ShapeDtypeStruct(tokens.shape, BF),...  57.8 us
    unnamed x4, local copies, waits for them, and re-layouts  3.01 us

profile of v2, /device:TPU:1, one launch (start us, length us, event | category | flops | bytes accessed | tf_op | source)
XLA Modules:
  0.0 61.4 jit_solution(3550036009067187080)
XLA Ops:
  0.6 57.8 %layer.1 = (bf16[20,2048]{1,0:T(8,128)(2,1)}, f32[20,8,64,128]{3,2,1,0:T(8,128)S(1)}) custom-call(bf16[20,2048]{1,0:T(8,128)(2,1)} %tokens_h.1, s32[1,20]{1,0:T(1,128)} %bitcast.13, f32[1,2048]{1,0:T(1,128)} %bitcast.8, f32[1,1024]{1,0:T(1,128)} %bitcast.10, f32[1,2048]{1,0:T(1,128)} %bitcast.9, s32[6,20]{1,0:T(8,128)} %bitcast.11, f32[6,20]{1,0:T(8,128)} %bitcast.12, ...), custom_call_target="tpu_custom_call" | custom-call | tf_op jit(solution)/shard_map/layer/pallas_call | solution.py:339
  58.4 0.0 copy-start
  58.4 2.4 %copy.19 = f32[20,8,64,128]{3,2,1,0:T(8,128)} copy(f32[20,8,64,128]{3,2,1,0:T(8,128)S(1)} %get-tuple-element.3) | data formatting | bytes 10485760
  60.8 0.0 copy-done
  60.8 0.6 %copy.20 = bf16[20,2048]{1,0:T(8,128)(2,1)} copy(bf16[20,2048]{1,0:T(8,128)(2,1)S(1)} %copy-done) | data formatting | bytes 163840
Async XLA Ops:
  58.4 2.4 %copy-start = (bf16[20,2048]{1,0:T(8,128)(2,1)S(1)}, bf16[20,2048]{1,0:T(8,128)(2,1)}, u32[]{:S(2)}) copy-start(bf16[20,2048]{1,0:T(8,128)(2,1)} %get-tuple-element.6) | copy-start | bytes 245764

commit v3 on v2

v3 whole, which is shorter than its diff:
```python
import math

import jax
import jax.numpy as jnp
from jax import lax
from jax.experimental import pallas as pl
from jax.experimental.pallas import tpu as pltpu
from jax.sharding import PartitionSpec as P

MESH = pl.DeviceIdType.MESH
EPS = 1e-06
BF = jnp.bfloat16
F32 = jnp.float32
STRIDES = (32, 8, 2)


def hops(d):
    return sum((0, 1, 2, 1)[k] for k in d[:3])


MOVES = [(z, y, x, c) for z in range(4) for y in range(4) for x in range(4) for c in range(2)]
MOVES = (lambda r: [(0, 0, 0, 0)] + r[0::2][:63] + r[1::2] + r[0::2][63:])(sorted([d for d in MOVES if d != (0, 0, 0, 0)], key=lambda d: (-hops(d), d)))


def kernel(
    tokens_h, pos_h, mixg_h, retg_h, ffng_h, routes_h, rw_h,
    state, wq, wk, wv, wo, eg, eu, ed,
    result, new_state,
    tokens, pos, mixg, retg, ffng, routes_t, rw_t, wqv, wkv, wvv, wh, egv, euv, edv,
    xin, tab, kq, ee, vt, rt, mix, att, att_in, lined, spread, nm, dmask, chl, rsd, xs, hid,
    send1, recv1, send2, recv2,
    lsem, ssem_in, ag_s, ag_r, ps, pr, a_s, a_r, b_s, b_r,
):
    me = lax.axis_index("ep")
    co = (me // 32, (me // 8) % 4, (me // 2) % 4)
    c = me % 2
    half = (co[0], co[1] // 2, co[2] // 2)
    own = (half[0] * 2 + half[1]) * 2 + half[2]
    n_tok = tokens.shape[0]

    def along(axis, d):
        return ((co[axis] + d) % 4 - co[axis]) * STRIDES[axis]

    line = [(me + along(0, d), ((half[0] + d) % 4, half[1], half[2])) for d in (2, 1, 3)]
    cross = [
        (me + along(1, 2 * fy) + along(2, 2 * fx), (half[0], (half[1] + fy) % 2, (half[2] + fx) % 2))
        for fy, fx in ((1, 1), (1, 0), (0, 1))
    ]

    low = (co[1] % 2, co[2] % 2, c)
    seat = low[0] * 4 + low[1] * 2 + c
    mates = []
    for flip in range(1, 8):
        f = (flip // 4, (flip // 2) % 2, flip % 2)
        there = me + sum(f[a] * (1 - 2 * low[a]) * (8, 2, 1)[a] for a in range(3))
        its_seat = seat + sum(f[a] * (1 - 2 * low[a]) * (4, 2, 1)[a] for a in range(3))
        mates.append((there, its_seat))

    bar = pltpu.get_barrier_semaphore()
    for there, _ in mates:
        pl.semaphore_signal(bar, inc=1, device_id=(there,), device_id_type=MESH)
    for there, _ in line + cross:
        pl.semaphore_signal(bar, inc=1, device_id=(there,), device_id_type=MESH)

    def fetch(n, src, dst):
        cp = pltpu.make_async_copy(src, dst, lsem.at[n])
        cp.start()
        return cp

    cp_tok = fetch(7, tokens_h, tokens)
    cp_mixg = fetch(8, mixg_h, mixg)
    cp_rt = fetch(9, routes_h, routes_t)
    cp_rw = fetch(10, rw_h, rw_t)
    cp_pos = fetch(11, pos_h, pos)
    cp_wo = fetch(0, wo, wh.at[own])
    cp_k = fetch(1, wk, wkv)
    cp_q = fetch(2, wq, wqv)
    cp_v = fetch(3, wv, wvv)

    def state_in(h):
        return pltpu.make_async_copy(state.at[:, h], new_state.at[:, h], ssem_in.at[h])

    for h in range(8):
        state_in(h).start()
    cp_retg = fetch(12, retg_h, retg)
    cp_ffng = fetch(13, ffng_h, ffng)
    cp_g = fetch(4, eg.at[0], egv)
    cp_u = fetch(5, eu.at[0], euv)
    cp_d = fetch(6, ed.at[0], edv)
    cp_rt.wait()
    cp_rw.wait()
    cp_pos.wait()

    tab[...] = jnp.full(tab.shape, -1, jnp.int32)
    tab[0:6, 0:n_tok] = routes_t[...]
    tab[8:9, 0:n_tok] = pos[...]
    wtab = jnp.concatenate([rw_t[...], jnp.zeros((6, 128 - n_tok), F32)], axis=1)
    rows = lax.broadcasted_iota(jnp.int32, (256, 128), 0)
    expert = rows // 2
    slot = (rows % 2).astype(F32)
    member = jnp.zeros((256, 128), F32)
    weight = jnp.zeros((256, 128), F32)
    for k in range(6):
        hit = tab[k : k + 1, :] == expert
        member = member + jnp.where(hit, 1.0, 0.0)
        weight = weight + jnp.where(hit, wtab[k : k + 1, :], 0.0)
    before = jnp.where(
        lax.broadcasted_iota(jnp.int32, (128, 128), 0) < lax.broadcasted_iota(jnp.int32, (128, 128), 1), 1.0, 0.0
    ).astype(BF)
    place = jnp.dot(member.astype(BF), before, preferred_element_type=F32)
    chosen = jnp.where(place == slot, member, 0.0)
    dmask[...] = chosen.astype(BF)
    comb = (chosen * weight).T
    high = comb.astype(BF)
    chl[0:32, :] = high[0:32, :]
    chl[32:64, :] = (comb - high.astype(F32)).astype(BF)[0:32, :]

    erow = lax.broadcasted_iota(jnp.int32, (128, 128), 0)
    etok = jnp.where(erow < 64, erow % 32, -1)
    for t in range(n_tok):
        ee[:, t * 128 : (t + 1) * 128] = jnp.where(etok == t, 1.0, 0.0).astype(BF)

    spots = tab[8:9, 0:32].astype(F32)
    freqs = jnp.exp(-math.log(10000.0) * lax.broadcasted_iota(jnp.int32, (32, 32), 0).astype(F32) / 32.0)
    angle = spots * freqs
    cosine = jnp.cos(angle)
    sine = jnp.sin(angle)

    cp_tok.wait()
    cp_mixg.wait()
    wide = tokens[...].astype(F32)
    scaled = wide * lax.rsqrt(jnp.mean(wide * wide, axis=-1, keepdims=True) + EPS)
    xin[...] = jnp.zeros(xin.shape, BF)
    xin[0:n_tok, :] = (scaled * mixg[...]).astype(BF)

    def send_block(cc, part, peers, sem):
        piece = wh.at[(cc[0] * 2 + cc[1]) * 2 + cc[2], :, pl.ds(part * 512, 512)]
        for there, _ in peers:
            pltpu.make_async_remote_copy(
                src_ref=piece, dst_ref=piece, send_sem=ag_s, recv_sem=ag_r.at[sem],
                device_id=(there,), device_id_type=MESH,
            ).start()

    def gathered(n, sem):
        seen = wh.at[pl.ds(0, n), :, pl.ds(0, 512)]
        pltpu.make_async_copy(seen, seen, ag_r.at[sem]).wait()

    def gather_start():
        send_block(half, 0, line, 0)
        send_block(half, 1, cross, 1)
        send_block(half, 0, cross, 2)
        send_block(half, 1, line, 3)

    def gather_forward():
        gathered(3, 0)
        for _, cc in line:
            send_block(cc, 0, cross, 2)
        gathered(3, 1)
        for _, cc in cross:
            send_block(cc, 1, line, 3)

    def project(wref, n):
        return jnp.dot(xin[...], wref[:, n * 256 : (n + 1) * 256], preferred_element_type=F32).astype(BF).astype(F32)

    def rotated(offset, wref, scale):
        for n in range(2):
            cols = project(wref, n).T
            for s in range(4):
                a = cols[s * 64 : s * 64 + 32, :]
                b = cols[s * 64 + 32 : s * 64 + 64, :]
                for first, value in ((0, a * cosine - b * sine), (32, b * cosine + a * sine)):
                    value = value * scale
                    high = value.astype(BF)
                    low_part = (value - high.astype(F32)).astype(BF)
                    kq[n * 4 + s, offset + first : offset + first + 32, :] = jnp.concatenate(
                        [high, low_part, jnp.zeros((32, 64), BF)], axis=1
                    )

    cp_k.wait()
    rotated(0, wkv, 0.125)
    pl.semaphore_wait(bar, 13)
    cp_wo.wait()
    gather_start()
    cp_q.wait()
    rotated(64, wqv, 1.0)
    cp_v.wait()
    for n in range(4):
        part = project(wvv, n)
        vt[2 * n] = part[:, 0:128]
        vt[2 * n + 1] = part[:, 128:256]

    def seven(buf, sem):
        seen = buf.at[pl.ds(0, 7), pl.ds(0, 24)]
        pltpu.make_async_copy(seen, seen, sem).wait()

    def two_heads(p):
        for h in (2 * p, 2 * p + 1):
            state_in(h).wait()
        lhs = kq[2 * p : 2 * p + 2].reshape(256, 128)
        for g in range(n_tok // 4):
            wide_kq = jnp.dot(lhs, ee[:, g * 512 : (g + 1) * 512], preferred_element_type=F32)
            for n, h in enumerate((2 * p, 2 * p + 1)):
                decay = 1.0 - 2.0 ** (-2 - h)
                for i in range(4):
                    t = g * 4 + i
                    key = wide_kq[n * 128 : n * 128 + 64, i * 128 : (i + 1) * 128]
                    query = wide_kq[n * 128 + 64 : n * 128 + 128, i * 128 : (i + 1) * 128]
                    new = decay * new_state[t, h] + key * vt[h, t : t + 1, :]
                    new_state[t, h] = new
                    rt[h, t : t + 1, :] = jnp.sum(query * new, axis=0, keepdims=True)
        for h in (2 * p, 2 * p + 1):
            read = rt[h, 0:n_tok, :]
            centred = read - jnp.mean(read, axis=-1, keepdims=True)
            normed = centred * lax.rsqrt(jnp.mean(centred * centred, axis=-1, keepdims=True) + EPS)
            mix[seat, 0:n_tok, h * 128 : (h + 1) * 128] = (normed * retg[:, h * 128 : (h + 1) * 128]).astype(BF)
        piece = mix.at[seat, pl.ds(0, 24), pl.ds(p * 256, 256)]
        for n, (there, _) in enumerate([mates[5], mates[3], mates[1], mates[0]]):
            pltpu.make_async_remote_copy(
                src_ref=piece, dst_ref=piece, send_sem=ps.at[0], recv_sem=pr.at[2 + n],
                device_id=(there,), device_id_type=MESH,
            ).start()

    cp_retg.wait()
    two_heads(0)
    two_heads(1)
    two_heads(2)
    gather_forward()
    two_heads(3)
    nm[...] = jnp.zeros(nm.shape, BF)

    srow = lax.broadcasted_iota(jnp.int32, (512, 128), 0)
    lane = lax.broadcasted_iota(jnp.int32, (512, 128), 1)
    target = (srow % 128) // 64 * 256 + (srow % 64) // 32 * 128 + (srow % 32) // 16 * 64 + srow // 128 * 16 + srow % 16
    for n in range(4):
        spread[:, n * 128 : (n + 1) * 128] = jnp.where(lane + n * 128 == target, 1.0, 0.0).astype(BF)

    for n, (_, its_seat) in ((1, mates[3]), (2, mates[1]), (0, mates[5])):
        block = mix.at[0, pl.ds(0, 24)]
        pltpu.make_async_copy(block, block, pr.at[2 + n]).wait()
        block = mix.at[its_seat, pl.ds(0, 24)]
        pltpu.make_async_remote_copy(
            src_ref=block, dst_ref=block, send_sem=ps.at[0], recv_sem=pr.at[0],
            device_id=(mates[0][0],), device_id_type=MESH,
        ).start()
    gathered(12, 2)
    gathered(12, 3)
    block = mix.at[0, pl.ds(0, 24)]
    pltpu.make_async_copy(block, block, pr.at[5]).wait()
    pltpu.make_async_copy(mix.at[pl.ds(0, 3), pl.ds(0, 24)], mix.at[pl.ds(0, 3), pl.ds(0, 24)], pr.at[0]).wait()
    att[...] = lax.dot_general(
        mix[...].reshape(256, 1024), wh[...].reshape(256, 1024), (((1,), (1,)), ((), ())), preferred_element_type=F32
    ).astype(BF).reshape(8, 32, 256)
    for there, its_seat in mates:
        pltpu.make_async_remote_copy(
            src_ref=att.at[its_seat, pl.ds(0, 24)], dst_ref=att_in.at[seat, pl.ds(0, 24)],
            send_sem=ps.at[1], recv_sem=pr.at[1], device_id=(there,), device_id_type=MESH,
        ).start()
    att_in[seat] = att[seat]
    seven(att_in, pr.at[1])
    for py in range(2):
        for zp in range(2):
            for s in range(4):
                lined[(py * 2 + zp) * 32 : (py * 2 + zp + 1) * 32, s * 128 : (s + 1) * 128] = att_in[
                    py * 4 + s, :, zp * 128 : (zp + 1) * 128
                ]
    attended = jnp.dot(lined[...], spread[...], preferred_element_type=F32)
    cp_ffng.wait()
    total = jnp.zeros((n_tok, 1), F32)
    for n in range(16):
        z, y = n // 4, n % 4
        first = (y % 2 * 2 + z // 2) * 32
        at = (z % 2 * 2 + y // 2) * 128
        cols = slice(n * 128, (n + 1) * 128)
        res = (tokens[:, cols].astype(F32) + attended[first : first + n_tok, at : at + 128]).astype(BF).astype(F32)
        rsd[:, cols] = res
        total = total + jnp.sum(res * res, axis=-1, keepdims=True)
    inv = lax.rsqrt(total / 2048.0 + EPS)
    nm[0:n_tok, :] = (rsd[...] * inv * ffng[...]).astype(BF)

    for n in range(8):
        cols = slice(n * 256, (n + 1) * 256)
        out = jnp.dot(dmask[:, 0:32], nm[:, cols], preferred_element_type=F32).astype(BF)
        send1[:, :, cols] = out.reshape(128, 2, 256)

    def peers(half, sign, put):
        zs = [(co[0] + sign * d) % 4 * 32 for d in range(4)]
        ys = [(co[1] + sign * d) % 4 * 8 for d in range(4)]
        xs4 = [(co[2] + sign * d) % 4 * 2 for d in range(4)]
        cs = [c, 1 - c]
        for j in range(max(1, half * 64), half * 64 + 64):
            d = MOVES[j]
            put(j, zs[d[0]] + ys[d[1]] + xs4[d[2]] + cs[d[3]])

    def dispatch(half):
        def put(j, t):
            pltpu.make_async_remote_copy(
                src_ref=send1.at[t], dst_ref=recv1.at[j], send_sem=a_s, recv_sem=a_r.at[half],
                device_id=(t,), device_id_type=MESH,
            ).start()

        peers(half, 1, put)

    def give_back(half):
        def put(j, t):
            pltpu.make_async_remote_copy(
                src_ref=send2.at[j], dst_ref=recv2.at[me], send_sem=b_s, recv_sem=b_r,
                device_id=(t,), device_id_type=MESH,
            ).start()

        peers(half, -1, put)

    def arrived(buf, first, count, sem):
        seen = buf.at[pl.ds(first, count)]
        pltpu.make_async_copy(seen, seen, sem).wait()

    def experts(half):
        base = half * 128
        for i in range(8):
            xs[base + i * 16 : base + (i + 1) * 16, :] = recv1[half * 64 + i * 8 : half * 64 + (i + 1) * 8].reshape(16, 2048)
        mine = slice(base, base + 128)
        for n in range(2):
            cols = slice(n * 256, (n + 1) * 256)
            gate = jnp.dot(xs[mine, :], egv[:, cols], preferred_element_type=F32)
            up = jnp.dot(xs[mine, :], euv[:, cols], preferred_element_type=F32)
            hid[mine, cols] = (jax.nn.silu(gate) * up).astype(BF)
        for n in range(8):
            cols = slice(n * 256, (n + 1) * 256)
            out = jnp.dot(hid[mine, :], edv[:, cols], preferred_element_type=F32).astype(BF)
            send2[half * 64 : half * 64 + 64, :, cols] = out.reshape(64, 2, 256)

    dispatch(0)
    dispatch(1)
    recv1[0] = send1[me]
    cp_g.wait()
    cp_u.wait()
    cp_d.wait()
    arrived(recv1, 1, 63, a_r.at[0])
    experts(0)
    give_back(0)
    recv2[me] = send2[0]
    arrived(recv1, 64, 64, a_r.at[1])
    experts(1)
    give_back(1)
    arrived(recv2, 0, 127, b_r)

    def unpack2(i, _):
        xs[pl.ds(i * 16, 16), :] = recv2[pl.ds(i * 8, 8)].reshape(16, 2048)
        return 0

    lax.fori_loop(0, 16, unpack2, 0)
    for n in range(8):
        cols = slice(n * 256, (n + 1) * 256)
        got = jnp.dot(chl[...], xs[:, cols], preferred_element_type=F32)
        result[:, cols] = (rsd[:, cols] + got[0:n_tok, :] + got[32 : 32 + n_tok, :]).astype(BF)

    arrived(send1, 0, 127, a_s)
    arrived(send2, 0, 127, b_s)
    sent = wh.at[pl.ds(0, 15)]
    pltpu.make_async_copy(sent, sent, ag_s).wait()
    seven(mix, ps.at[0])
    seven(att, ps.at[1])


def shards(
    tokens, positions, state, mix_gain, w_query, w_key, w_value, ret_gain, w_out, ffn_gain,
    routes, route_weights, expert_gate, expert_up, expert_down,
):
    vmem = pl.BlockSpec(memory_space=pltpu.VMEM)
    hbm = pl.BlockSpec(memory_space=pl.ANY)
    n_tok = tokens.shape[0]
    dma = pltpu.SemaphoreType.DMA
    vm = pltpu.VMEM
    return pl.pallas_call(
        kernel,
        out_shape=(
            jax.ShapeDtypeStruct(tokens.shape, BF),
            pltpu.VMEM(state.shape, F32),
        ),
        in_specs=[hbm] * 15,
        out_specs=(vmem, vmem),
        scratch_shapes=[
            vm((n_tok, 2048), BF), vm((1, n_tok), jnp.int32), vm((1, 2048), F32), vm((1, 1024), F32), vm((1, 2048), F32),
            vm((6, n_tok), jnp.int32), vm((6, n_tok), F32),
            vm((2048, 512), BF), vm((2048, 512), BF), vm((2048, 1024), BF),
            vm((16, 16, 1024), BF), vm((2048, 512), BF), vm((2048, 512), BF), vm((512, 2048), BF),
            vm((32, 2048), BF), vm((16, 128), jnp.int32), vm((8, 128, 128), BF), vm((128, n_tok * 128), BF),
            vm((8, 32, 128), F32), vm((8, 32, 128), F32), vm((8, 32, 1024), BF),
            vm((8, 32, 256), BF), vm((8, 32, 256), BF), vm((128, 512), BF), vm((512, 512), BF), vm((32, 2048), BF), vm((256, 128), BF), vm((64, 256), BF),
            vm((n_tok, 2048), F32), vm((256, 2048), BF), vm((256, 512), BF),
            vm((128, 2, 2048), BF), vm((128, 2, 2048), BF), vm((128, 2, 2048), BF), vm((128, 2, 2048), BF),
            dma((14,)), dma((8,)), dma, dma((4,)), dma((2,)), dma((6,)), dma, dma((2,)), dma, dma,
        ],
        compiler_params=pltpu.CompilerParams(collective_id=0, has_side_effects=True, vmem_limit_bytes=61718528),
        name="layer",
    )(
        tokens, positions.reshape(1, n_tok), mix_gain.reshape(1, -1), ret_gain.reshape(1, -1), ffn_gain.reshape(1, -1),
        routes.T, route_weights.T, state, w_query, w_key, w_value, w_out.T, expert_gate, expert_up, expert_down,
    )


def solution(mesh):
    placed = (
        P("ep", None), P("ep"), P("ep", None, None, None), P(), P(), P(), P(), P(), P(None, "ep"), P(),
        P("ep", None), P("ep", None), P("ep", None, None), P("ep", None, None), P("ep", None, None),
    )
    return jax.shard_map(
        shards, mesh=mesh, in_specs=placed, out_specs=(P("ep", None), P("ep", None, None, None)), check_vma=False
    )
```

time: 61.5 us -> 55.6 us (0.904)
  Pallas kernels: 57.8 us -> 51.8 us
    pallas_call x1, Pallas kernels: 57.8 us -> 51.8 us  [shards(): pl.pallas_call(kernel, out_shape=(jax.ShapeDtypeStruct(tokens.shape, BF),...]
where the time goes in v3:
time: 55.6 us; the launch traced here: 55.5 us
  Pallas kernels  51.8 us (93%)
  local copies, waits for them, and re-layouts  3.01 us (5%)
  between operations  0.65 us (1%)
    pallas_call x1, Pallas kernels, shards(): pl.pallas_call(kernel, out_shape=(jax.ShapeDtypeStruct(tokens.shape, BF),...  51.8 us
    unnamed x4, local copies, waits for them, and re-layouts  3.01 us

profile of v3, /device:TPU:1, one launch (start us, length us, event | category | flops | bytes accessed | tf_op | source)
XLA Modules:
  0.0 55.5 jit_solution(1719658732465846844)
XLA Ops:
  0.6 51.8 %layer.1 = (bf16[20,2048]{1,0:T(8,128)(2,1)}, f32[20,8,64,128]{3,2,1,0:T(8,128)S(1)}) custom-call(bf16[20,2048]{1,0:T(8,128)(2,1)} %tokens_h.1, s32[1,20]{1,0:T(1,128)} %bitcast.13, f32[1,2048]{1,0:T(1,128)} %bitcast.8, f32[1,1024]{1,0:T(1,128)} %bitcast.10, f32[1,2048]{1,0:T(1,128)} %bitcast.9, s32[6,20]{1,0:T(8,128)} %bitcast.11, f32[6,20]{1,0:T(8,128)} %bitcast.12, ...), custom_call_target="tpu_custom_call" | custom-call | tf_op jit(solution)/shard_map/layer/pallas_call | solution.py:373
  52.5 0.0 copy-start
  52.5 2.4 %copy.19 = f32[20,8,64,128]{3,2,1,0:T(8,128)} copy(f32[20,8,64,128]{3,2,1,0:T(8,128)S(1)} %get-tuple-element.3) | data formatting | bytes 10485760
  54.8 0.0 copy-done
  54.8 0.6 %copy.20 = bf16[20,2048]{1,0:T(8,128)(2,1)} copy(bf16[20,2048]{1,0:T(8,128)(2,1)S(1)} %copy-done) | data formatting | bytes 163840
Async XLA Ops:
  52.5 2.4 %copy-start = (bf16[20,2048]{1,0:T(8,128)(2,1)S(1)}, bf16[20,2048]{1,0:T(8,128)(2,1)}, u32[]{:S(2)}) copy-start(bf16[20,2048]{1,0:T(8,128)(2,1)} %get-tuple-element.6) | copy-start | bytes 245764

commit v4 on v3

--- a/solution.py
+++ b/solution.py
@@ -18,8 +18,17 @@
     return sum((0, 1, 2, 1)[k] for k in d[:3])
 
 
-MOVES = [(z, y, x, c) for z in range(4) for y in range(4) for x in range(4) for c in range(2)]
-MOVES = (lambda r: [(0, 0, 0, 0)] + r[0::2][:63] + r[1::2] + r[0::2][63:])(sorted([d for d in MOVES if d != (0, 0, 0, 0)], key=lambda d: (-hops(d), d)))
+LINES = (
+    (0, 0), (2, 2), (2, 1), (3, 2), (1, 1), (3, 3), (1, 0), (0, 3),
+    (2, 3), (1, 2), (2, 0), (0, 2), (1, 3), (3, 1), (3, 0), (0, 1),
+)
+MOVES = [
+    sorted(
+        [(l, *LINES[l], x, c) for l in range(n * 8, n * 8 + 8) for x in range(4) for c in range(2) if LINES[l] + (x, c) != (0,) * 4],
+        key=lambda d: (-hops(d[1:]), d),
+    )
+    for n in range(2)
+]
 
 
 def kernel(
@@ -27,37 +36,29 @@
     state, wq, wk, wv, wo, eg, eu, ed,
     result, new_state,
     tokens, pos, mixg, retg, ffng, routes_t, rw_t, wqv, wkv, wvv, wh, egv, euv, edv,
-    xin, tab, kq, ee, vt, rt, mix, att, att_in, lined, spread, nm, dmask, chl, rsd, xs, hid,
+    xin, tab, kq, ee, vt, rt, mix, res_out, res_in, tok_out, tok_in, lined, spread, sorted_in, gains, plan, dall, xq, chl, rsd, xs, hid,
     send1, recv1, send2, recv2,
     lsem, ssem_in, ag_s, ag_r, ps, pr, a_s, a_r, b_s, b_r,
 ):
     me = lax.axis_index("ep")
     co = (me // 32, (me // 8) % 4, (me // 2) % 4)
     c = me % 2
-    half = (co[0], co[1] // 2, co[2] // 2)
-    own = (half[0] * 2 + half[1]) * 2 + half[2]
+    own = co[0] * 4 + co[1]
     n_tok = tokens.shape[0]
 
     def along(axis, d):
         return ((co[axis] + d) % 4 - co[axis]) * STRIDES[axis]
 
-    line = [(me + along(0, d), ((half[0] + d) % 4, half[1], half[2])) for d in (2, 1, 3)]
-    cross = [
-        (me + along(1, 2 * fy) + along(2, 2 * fx), (half[0], (half[1] + fy) % 2, (half[2] + fx) % 2))
-        for fy, fx in ((1, 1), (1, 0), (0, 1))
-    ]
-
-    low = (co[1] % 2, co[2] % 2, c)
-    seat = low[0] * 4 + low[1] * 2 + c
-    mates = []
-    for flip in range(1, 8):
-        f = (flip // 4, (flip // 2) % 2, flip % 2)
-        there = me + sum(f[a] * (1 - 2 * low[a]) * (8, 2, 1)[a] for a in range(3))
-        its_seat = seat + sum(f[a] * (1 - 2 * low[a]) * (4, 2, 1)[a] for a in range(3))
-        mates.append((there, its_seat))
+    line = [(me + along(0, d), ((co[0] + d) % 4, co[1])) for d in (2, 1, 3)]
+    cross = [(me + along(1, d), (co[0], (co[1] + d) % 4)) for d in (2, 1, 3)]
+
+    seat = co[2] * 2 + c
+    mates = [(me + along(2, d), (co[2] + d) % 4 * 2 + c) for d in (2, 1, 3)]
+    mates.append((me + 1 - 2 * c, seat + 1 - 2 * c))
+    others = mates + [(there + 1 - 2 * c, its_seat + 1 - 2 * c) for there, its_seat in mates[:3]]
 
     bar = pltpu.get_barrier_semaphore()
-    for there, _ in mates:
+    for there, _ in others:
         pl.semaphore_signal(bar, inc=1, device_id=(there,), device_id_type=MESH)
     for there, _ in line + cross:
         pl.semaphore_signal(bar, inc=1, device_id=(there,), device_id_type=MESH)
@@ -80,13 +81,10 @@
     def state_in(h):
         return pltpu.make_async_copy(state.at[:, h], new_state.at[:, h], ssem_in.at[h])
 
-    for h in range(8):
+    for h in range(4):
         state_in(h).start()
     cp_retg = fetch(12, retg_h, retg)
     cp_ffng = fetch(13, ffng_h, ffng)
-    cp_g = fetch(4, eg.at[0], egv)
-    cp_u = fetch(5, eu.at[0], euv)
-    cp_d = fetch(6, ed.at[0], edv)
     cp_rt.wait()
     cp_rw.wait()
     cp_pos.wait()
@@ -109,7 +107,8 @@
     ).astype(BF)
     place = jnp.dot(member.astype(BF), before, preferred_element_type=F32)
     chosen = jnp.where(place == slot, member, 0.0)
-    dmask[...] = chosen.astype(BF)
+    plan[seat] = jnp.full((8, 128), -1.0, F32)
+    plan[seat, 0:6, 0:n_tok] = routes_t[...].astype(F32)
     comb = (chosen * weight).T
     high = comb.astype(BF)
     chl[0:32, :] = high[0:32, :]
@@ -134,7 +133,7 @@
     xin[0:n_tok, :] = (scaled * mixg[...]).astype(BF)
 
     def send_block(cc, part, peers, sem):
-        piece = wh.at[(cc[0] * 2 + cc[1]) * 2 + cc[2], :, pl.ds(part * 512, 512)]
+        piece = wh.at[cc[0] * 4 + cc[1], :, pl.ds(part * 512, 512)]
         for there, _ in peers:
             pltpu.make_async_remote_copy(
                 src_ref=piece, dst_ref=piece, send_sem=ag_s, recv_sem=ag_r.at[sem],
@@ -146,10 +145,11 @@
         pltpu.make_async_copy(seen, seen, ag_r.at[sem]).wait()
 
     def gather_start():
-        send_block(half, 0, line, 0)
-        send_block(half, 1, cross, 1)
-        send_block(half, 0, cross, 2)
-        send_block(half, 1, line, 3)
+        here = (co[0], co[1])
+        send_block(here, 0, line, 0)
+        send_block(here, 1, cross, 1)
+        send_block(here, 0, cross, 2)
+        send_block(here, 1, line, 3)
 
     def gather_forward():
         gathered(3, 0)
@@ -181,6 +181,13 @@
     pl.semaphore_wait(bar, 13)
     cp_wo.wait()
     gather_start()
+    for there, _ in others:
+        pltpu.make_async_remote_copy(
+            src_ref=plan.at[seat], dst_ref=plan.at[seat], send_sem=ps.at[3], recv_sem=pr.at[7],
+            device_id=(there,), device_id_type=MESH,
+        ).start()
+    for h in range(4, 8):
+        state_in(h).start()
     cp_q.wait()
     rotated(64, wqv, 1.0)
     cp_v.wait()
@@ -214,9 +221,9 @@
             normed = centred * lax.rsqrt(jnp.mean(centred * centred, axis=-1, keepdims=True) + EPS)
             mix[seat, 0:n_tok, h * 128 : (h + 1) * 128] = (normed * retg[:, h * 128 : (h + 1) * 128]).astype(BF)
         piece = mix.at[seat, pl.ds(0, 24), pl.ds(p * 256, 256)]
-        for n, (there, _) in enumerate([mates[5], mates[3], mates[1], mates[0]]):
+        for n, (there, _) in enumerate(mates):
             pltpu.make_async_remote_copy(
-                src_ref=piece, dst_ref=piece, send_sem=ps.at[0], recv_sem=pr.at[2 + n],
+                src_ref=piece, dst_ref=piece, send_sem=ps.at[0], recv_sem=pr.at[2 + (0, 2, 1, 3)[n]],
                 device_id=(there,), device_id_type=MESH,
             ).start()
 
@@ -226,84 +233,105 @@
     two_heads(2)
     gather_forward()
     two_heads(3)
-    nm[...] = jnp.zeros(nm.shape, BF)
-
-    srow = lax.broadcasted_iota(jnp.int32, (512, 128), 0)
-    lane = lax.broadcasted_iota(jnp.int32, (512, 128), 1)
-    target = (srow % 128) // 64 * 256 + (srow % 64) // 32 * 128 + (srow % 32) // 16 * 64 + srow // 128 * 16 + srow % 16
-    for n in range(4):
+    cp_g = fetch(4, eg.at[0], egv)
+    cp_u = fetch(5, eu.at[0], euv)
+    cp_d = fetch(6, ed.at[0], edv)
+
+    srow = lax.broadcasted_iota(jnp.int32, (1024, 128), 0)
+    lane = lax.broadcasted_iota(jnp.int32, (1024, 128), 1)
+    target = srow % 128 // 16 * 128 + srow // 128 * 16 + srow % 16
+    for n in range(8):
         spread[:, n * 128 : (n + 1) * 128] = jnp.where(lane + n * 128 == target, 1.0, 0.0).astype(BF)
 
-    for n, (_, its_seat) in ((1, mates[3]), (2, mates[1]), (0, mates[5])):
+    cp_ffng.wait()
+    sorted_in[0:n_tok, :] = tokens[:, 0:1024]
+    sorted_in[32 : 32 + n_tok, :] = tokens[:, 1024:2048]
+    rows = []
+    for n in range(2):
+        rest = ffng[:, n * 1024 : (n + 1) * 1024]
+        for _ in range(3):
+            piece = rest.astype(BF).astype(F32)
+            rows.append(piece)
+            rest = rest - piece
+    rows.append(jnp.zeros((10, 1024), F32))
+    sorted_in[64:80, :] = jnp.concatenate(rows, axis=0).astype(BF)
+    by_core = lax.dot_general(sorted_in[...], spread[...], (((1,), (1,)), ((), ())), preferred_element_type=F32)
+    for g in range(8):
+        for n in range(2):
+            part = by_core[:, g * 128 : (g + 1) * 128]
+            tok_out[g, :, n * 128 : (n + 1) * 128] = part[n * 32 : n * 32 + 32, :].astype(BF)
+            at = 64 + 3 * n
+            gains[g : g + 1, n * 128 : (n + 1) * 128] = part[at : at + 1, :] + part[at + 1 : at + 2, :] + part[at + 2 : at + 3, :]
+    for there, its_seat in others:
+        pltpu.make_async_remote_copy(
+            src_ref=tok_out.at[its_seat, pl.ds(0, 24)], dst_ref=tok_in.at[seat, pl.ds(0, 24)],
+            send_sem=ps.at[2], recv_sem=pr.at[6], device_id=(there,), device_id_type=MESH,
+        ).start()
+    tok_in[seat] = tok_out[seat]
+    for n in (1, 2, 0):
+        its_seat = mates[n][1]
         block = mix.at[0, pl.ds(0, 24)]
         pltpu.make_async_copy(block, block, pr.at[2 + n]).wait()
         block = mix.at[its_seat, pl.ds(0, 24)]
         pltpu.make_async_remote_copy(
             src_ref=block, dst_ref=block, send_sem=ps.at[0], recv_sem=pr.at[0],
-            device_id=(mates[0][0],), device_id_type=MESH,
+            device_id=(mates[3][0],), device_id_type=MESH,
         ).start()
+    routed = plan.at[pl.ds(0, 7)]
+    pltpu.make_async_copy(routed, routed, pr.at[7]).wait()
+    ids = jnp.concatenate([plan[g, :, 0:32] for g in range(8)], axis=1)
+    mrow = lax.broadcasted_iota(jnp.int32, (256, 256), 0)
+    mlane = lax.broadcasted_iota(jnp.int32, (256, 256), 1)
+    mine_f = jnp.where(mrow % 16 // 2 == mlane // 32, 1.0, 0.0)
+    slot_f = (mrow % 2).astype(F32)
+    expert_f = (mrow // 16).astype(F32)
+    earlier = jnp.where(mrow < mlane, 1.0, 0.0).astype(BF)
+    for b in range(8):
+        member = jnp.zeros((256, 256), F32)
+        shifted_ids = ids - 16.0 * b
+        for k in range(6):
+            member = jnp.where(shifted_ids[k : k + 1, :] == expert_f, mine_f, member)
+        place = jnp.dot(member.astype(BF), earlier, preferred_element_type=F32)
+        dall[b * 256 : (b + 1) * 256, :] = jnp.where(place == slot_f, member, 0.0).astype(BF)
     gathered(12, 2)
     gathered(12, 3)
     block = mix.at[0, pl.ds(0, 24)]
     pltpu.make_async_copy(block, block, pr.at[5]).wait()
     pltpu.make_async_copy(mix.at[pl.ds(0, 3), pl.ds(0, 24)], mix.at[pl.ds(0, 3), pl.ds(0, 24)], pr.at[0]).wait()
-    att[...] = lax.dot_general(
+    seven(tok_in, pr.at[6])
+    attended = lax.dot_general(
         mix[...].reshape(256, 1024), wh[...].reshape(256, 1024), (((1,), (1,)), ((), ())), preferred_element_type=F32
-    ).astype(BF).reshape(8, 32, 256)
-    for there, its_seat in mates:
-        pltpu.make_async_remote_copy(
-            src_ref=att.at[its_seat, pl.ds(0, 24)], dst_ref=att_in.at[seat, pl.ds(0, 24)],
-            send_sem=ps.at[1], recv_sem=pr.at[1], device_id=(there,), device_id_type=MESH,
-        ).start()
-    att_in[seat] = att[seat]
-    seven(att_in, pr.at[1])
-    for py in range(2):
-        for zp in range(2):
-            for s in range(4):
-                lined[(py * 2 + zp) * 32 : (py * 2 + zp + 1) * 32, s * 128 : (s + 1) * 128] = att_in[
-                    py * 4 + s, :, zp * 128 : (zp + 1) * 128
-                ]
-    attended = jnp.dot(lined[...], spread[...], preferred_element_type=F32)
-    cp_ffng.wait()
-    total = jnp.zeros((n_tok, 1), F32)
-    for n in range(16):
-        z, y = n // 4, n % 4
-        first = (y % 2 * 2 + z // 2) * 32
-        at = (z % 2 * 2 + y // 2) * 128
-        cols = slice(n * 128, (n + 1) * 128)
-        res = (tokens[:, cols].astype(F32) + attended[first : first + n_tok, at : at + 128]).astype(BF).astype(F32)
-        rsd[:, cols] = res
-        total = total + jnp.sum(res * res, axis=-1, keepdims=True)
-    inv = lax.rsqrt(total / 2048.0 + EPS)
-    nm[0:n_tok, :] = (rsd[...] * inv * ffng[...]).astype(BF)
-
-    for n in range(8):
-        cols = slice(n * 256, (n + 1) * 256)
-        out = jnp.dot(dmask[:, 0:32], nm[:, cols], preferred_element_type=F32).astype(BF)
-        send1[:, :, cols] = out.reshape(128, 2, 256)
+    ).astype(BF).astype(F32)
+    piece = (tok_in[...].reshape(256, 256).astype(F32) + attended).astype(BF).astype(F32)
+    real = lax.broadcasted_iota(jnp.int32, (256, 256), 0) % 32 < n_tok
+    piece = jnp.where(real, piece, 0.0).astype(BF)
+    res_out[...] = piece.reshape(8, 32, 256)
+    for b in range(8):
+        out = jnp.dot(dall[b * 256 : (b + 1) * 256, :], piece, preferred_element_type=F32)
+        send1[b * 16 : (b + 1) * 16] = out.astype(BF).reshape(16, 16, 256)
 
     def peers(half, sign, put):
         zs = [(co[0] + sign * d) % 4 * 32 for d in range(4)]
         ys = [(co[1] + sign * d) % 4 * 8 for d in range(4)]
         xs4 = [(co[2] + sign * d) % 4 * 2 for d in range(4)]
         cs = [c, 1 - c]
-        for j in range(max(1, half * 64), half * 64 + 64):
-            d = MOVES[j]
-            put(j, zs[d[0]] + ys[d[1]] + xs4[d[2]] + cs[d[3]])
+        for l, dz, dy, dx, dc in MOVES[half]:
+            its_seat = xs4[dx] + cs[dc]
+            put(l, its_seat, zs[dz] + ys[dy] + its_seat)
 
     def dispatch(half):
-        def put(j, t):
+        def put(l, its_seat, t):
             pltpu.make_async_remote_copy(
-                src_ref=send1.at[t], dst_ref=recv1.at[j], send_sem=a_s, recv_sem=a_r.at[half],
+                src_ref=send1.at[t], dst_ref=recv1.at[seat, pl.ds(l * 16, 16)], send_sem=a_s, recv_sem=a_r.at[half],
                 device_id=(t,), device_id_type=MESH,
             ).start()
 
         peers(half, 1, put)
 
     def give_back(half):
-        def put(j, t):
+        def put(l, its_seat, t):
             pltpu.make_async_remote_copy(
-                src_ref=send2.at[j], dst_ref=recv2.at[me], send_sem=b_s, recv_sem=b_r,
+                src_ref=send2.at[l * 8 + its_seat], dst_ref=recv2.at[me], send_sem=b_s, recv_sem=b_r,
                 device_id=(t,), device_id_type=MESH,
             ).start()
 
@@ -314,14 +342,26 @@
         pltpu.make_async_copy(seen, seen, sem).wait()
 
     def experts(half):
-        base = half * 128
-        for i in range(8):
-            xs[base + i * 16 : base + (i + 1) * 16, :] = recv1[half * 64 + i * 8 : half * 64 + (i + 1) * 8].reshape(16, 2048)
-        mine = slice(base, base + 128)
+        mine = slice(half * 128, half * 128 + 128)
+        square = jnp.zeros((128, 128), F32)
+        for g in range(8):
+            value = recv1[g, mine, :].astype(F32)
+            value = value * value
+            square = square + value[:, 0:128] + value[:, 128:256]
+        inv = lax.rsqrt(jnp.sum(square, axis=-1, keepdims=True) / 2048.0 + EPS)
+        for g in range(8):
+            xq[g] = (recv1[g, mine, :].astype(F32) * inv * gains[g : g + 1, :]).astype(BF)
+
+        def rows_of(ref, g, cols):
+            return jnp.concatenate([ref[n * 128 + g * 16 : n * 128 + g * 16 + 16, cols] for n in range(16)], axis=0)
+
         for n in range(2):
             cols = slice(n * 256, (n + 1) * 256)
-            gate = jnp.dot(xs[mine, :], egv[:, cols], preferred_element_type=F32)
-            up = jnp.dot(xs[mine, :], euv[:, cols], preferred_element_type=F32)
+            gate = jnp.zeros((128, 256), F32)
+            up = jnp.zeros((128, 256), F32)
+            for g in range(8):
+                gate = gate + jnp.dot(xq[g], rows_of(egv, g, cols), preferred_element_type=F32)
+                up = up + jnp.dot(xq[g], rows_of(euv, g, cols), preferred_element_type=F32)
             hid[mine, cols] = (jax.nn.silu(gate) * up).astype(BF)
         for n in range(8):
             cols = slice(n * 256, (n + 1) * 256)
@@ -330,17 +370,30 @@
 
     dispatch(0)
     dispatch(1)
-    recv1[0] = send1[me]
+    recv1[seat, 0:16, :] = send1[me]
+    for there, its_seat in others:
+        pltpu.make_async_remote_copy(
+            src_ref=res_out.at[its_seat, pl.ds(0, 24)], dst_ref=res_in.at[seat, pl.ds(0, 24)],
+            send_sem=ps.at[1], recv_sem=pr.at[1], device_id=(there,), device_id_type=MESH,
+        ).start()
+    res_in[seat] = res_out[seat]
     cp_g.wait()
     cp_u.wait()
     cp_d.wait()
-    arrived(recv1, 1, 63, a_r.at[0])
+    arrived(send1, 0, 63, a_r.at[0])
     experts(0)
     give_back(0)
-    recv2[me] = send2[0]
-    arrived(recv1, 64, 64, a_r.at[1])
+    recv2[me] = send2[seat]
+    arrived(send1, 0, 64, a_r.at[1])
     experts(1)
     give_back(1)
+    seven(res_in, pr.at[1])
+    for n in range(2):
+        for g in range(8):
+            lined[n * 32 : (n + 1) * 32, g * 128 : (g + 1) * 128] = res_in[g, :, n * 128 : (n + 1) * 128]
+    resid = jnp.dot(lined[...], spread[...], preferred_element_type=F32)
+    rsd[:, 0:1024] = resid[0:n_tok, :]
+    rsd[:, 1024:2048] = resid[32 : 32 + n_tok, :]
     arrived(recv2, 0, 127, b_r)
 
     def unpack2(i, _):
@@ -358,7 +411,20 @@
     sent = wh.at[pl.ds(0, 15)]
     pltpu.make_async_copy(sent, sent, ag_s).wait()
     seven(mix, ps.at[0])
-    seven(att, ps.at[1])
+    seven(res_out, ps.at[1])
+    seven(tok_out, ps.at[2])
+    pltpu.make_async_copy(routed, routed, ps.at[3]).wait()
+
+
+def hand_over(result, new_state, result_out, state_out, sems):
+    copies = [pltpu.make_async_copy(result, result_out, sems.at[10])]
+    for n in range(10):
+        rows = pl.ds(n * 2, 2)
+        copies.append(pltpu.make_async_copy(new_state.at[rows], state_out.at[rows], sems.at[n]))
+    for cp in copies:
+        cp.start()
+    for cp in copies:
+        cp.wait()
 
 
 def shards(
@@ -370,10 +436,10 @@
     n_tok = tokens.shape[0]
     dma = pltpu.SemaphoreType.DMA
     vm = pltpu.VMEM
-    return pl.pallas_call(
+    result, new_state = pl.pallas_call(
         kernel,
         out_shape=(
-            jax.ShapeDtypeStruct(tokens.shape, BF),
+            pltpu.VMEM(tokens.shape, BF),
             pltpu.VMEM(state.shape, F32),
         ),
         in_specs=[hbm] * 15,
@@ -385,17 +451,28 @@
             vm((16, 16, 1024), BF), vm((2048, 512), BF), vm((2048, 512), BF), vm((512, 2048), BF),
             vm((32, 2048), BF), vm((16, 128), jnp.int32), vm((8, 128, 128), BF), vm((128, n_tok * 128), BF),
             vm((8, 32, 128), F32), vm((8, 32, 128), F32), vm((8, 32, 1024), BF),
-            vm((8, 32, 256), BF), vm((8, 32, 256), BF), vm((128, 512), BF), vm((512, 512), BF), vm((32, 2048), BF), vm((256, 128), BF), vm((64, 256), BF),
+            vm((8, 32, 256), BF), vm((8, 32, 256), BF), vm((8, 32, 256), BF), vm((8, 32, 256), BF),
+            vm((64, 1024), BF), vm((1024, 1024), BF), vm((80, 1024), BF), vm((8, 256), F32), vm((8, 8, 128), F32),
+            vm((2048, 256), BF), vm((8, 128, 256), BF), vm((64, 256), BF),
             vm((n_tok, 2048), F32), vm((256, 2048), BF), vm((256, 512), BF),
-            vm((128, 2, 2048), BF), vm((128, 2, 2048), BF), vm((128, 2, 2048), BF), vm((128, 2, 2048), BF),
-            dma((14,)), dma((8,)), dma, dma((4,)), dma((2,)), dma((6,)), dma, dma((2,)), dma, dma,
+            vm((128, 16, 256), BF), vm((8, 256, 256), BF), vm((128, 2, 2048), BF), vm((128, 2, 2048), BF),
+            dma((14,)), dma((8,)), dma, dma((4,)), dma((4,)), dma((8,)), dma, dma((2,)), dma, dma,
         ],
-        compiler_params=pltpu.CompilerParams(collective_id=0, has_side_effects=True, vmem_limit_bytes=61718528),
+        compiler_params=pltpu.CompilerParams(collective_id=0, has_side_effects=True, vmem_limit_bytes=61650000),
         name="layer",
     )(
         tokens, positions.reshape(1, n_tok), mix_gain.reshape(1, -1), ret_gain.reshape(1, -1), ffn_gain.reshape(1, -1),
         routes.T, route_weights.T, state, w_query, w_key, w_value, w_out.T, expert_gate, expert_up, expert_down,
     )
+    return pl.pallas_call(
+        hand_over,
+        out_shape=(jax.ShapeDtypeStruct(tokens.shape, BF), jax.ShapeDtypeStruct(state.shape, F32)),
+        in_specs=[vmem] * 2,
+        out_specs=(hbm, hbm),
+        scratch_shapes=[dma((11,))],
+        compiler_params=pltpu.CompilerParams(vmem_limit_bytes=1 << 20),
+        name="hand_over",
+    )(result, new_state)
 
 
 def solution(mesh):

time: 55.6 us -> 51.4 us (0.924)
  local copies, waits for them, and re-layouts: 3.01 us -> 0 us
  Pallas kernels: 51.8 us -> 50.7 us
    unnamed x4 -> x0, local copies, waits for them, and re-layouts: 3.01 us -> none
    pallas_call x1 -> x2, Pallas kernels: 51.8 us -> 50.7 us  [the longest x1 48.2 us: shards(): pl.pallas_call(kernel, out_shape=(pltpu.VMEM(tokens.shape, BF), pltpu.VME...]
where the time goes in v4:
time: 51.4 us; the launch traced here: 51.3 us
  Pallas kernels  50.7 us (99%)
  between operations  0.64 us (1%)
    pallas_call x1, Pallas kernels, shards(): pl.pallas_call(kernel, out_shape=(pltpu.VMEM(tokens.shape, BF), pltpu.VME...  48.2 us
    pallas_call x1, Pallas kernels, shards(): pl.pallas_call(hand_over, out_shape=(jax.ShapeDtypeStruct(tokens.shape, B...  2.46 us

profile of v4, /device:TPU:1, one launch (start us, length us, event | category | flops | bytes accessed | tf_op | source)
XLA Modules:
  0.0 51.3 jit_solution(18285364545926414460)
XLA Ops:
  0.6 48.2 %layer.1 = (bf16[20,2048]{1,0:T(8,128)(2,1)S(1)}, f32[20,8,64,128]{3,2,1,0:T(8,128)S(1)}) custom-call(bf16[20,2048]{1,0:T(8,128)(2,1)} %tokens_h.1, s32[1,20]{1,0:T(1,128)} %bitcast.13, f32[1,2048]{1,0:T(1,128)} %bitcast.8, f32[1,1024]{1,0:T(1,128)} %bitcast.10, f32[1,2048]{1,0:T(1,128)} %bitcast.9, s32[6,20]{1,0:T(8,128)} %bitcast.11, f32[6,20]{1,0:T(8,128)} %bitcast.12, ...), custom_call_target="tpu_custom_call" | custom-call | tf_op jit(solution)/shard_map/layer/pallas_call | solution.py:439
  48.9 2.5 %hand_over.1 = (bf16[20,2048]{1,0:T(8,128)(2,1)}, f32[20,8,64,128]{3,2,1,0:T(8,128)}) custom-call(bf16[20,2048]{1,0:T(8,128)(2,1)S(1)} %get-tuple-element.4.result, f32[20,8,64,128]{3,2,1,0:T(8,128)S(1)} %get-tuple-element.5.new_state), custom_call_target="tpu_custom_call" | custom-call | tf_op jit(solution)/shard_map/hand_over/pallas_call | solution.py:467

commit v5 on v4

--- a/solution.py
+++ b/solution.py
@@ -22,12 +22,13 @@
     (0, 0), (2, 2), (2, 1), (3, 2), (1, 1), (3, 3), (1, 0), (0, 3),
     (2, 3), (1, 2), (2, 0), (0, 2), (1, 3), (3, 1), (3, 0), (0, 1),
 )
+BOUNDS = (0, 8, 16)
 MOVES = [
     sorted(
-        [(l, *LINES[l], x, c) for l in range(n * 8, n * 8 + 8) for x in range(4) for c in range(2) if LINES[l] + (x, c) != (0,) * 4],
-        key=lambda d: (-hops(d[1:]), d),
+        [(l, *LINES[l], x, c) for l in range(a, b) for x in range(4) for c in range(2) if LINES[l] + (x, c) != (0,) * 4],
+        key=lambda d: (-hops(d[1:]), d[3], -d[0], d[4]),
     )
-    for n in range(2)
+    for a, b in zip(BOUNDS[:-1], BOUNDS[1:])
 ]
 
 
@@ -342,34 +343,35 @@
         pltpu.make_async_copy(seen, seen, sem).wait()
 
     def experts(half):
-        mine = slice(half * 128, half * 128 + 128)
-        square = jnp.zeros((128, 128), F32)
+        first, n_rows = BOUNDS[half] * 16, (BOUNDS[half + 1] - BOUNDS[half]) * 16
+        mine = slice(first, first + n_rows)
+        square = jnp.zeros((n_rows, 128), F32)
         for g in range(8):
             value = recv1[g, mine, :].astype(F32)
             value = value * value
             square = square + value[:, 0:128] + value[:, 128:256]
         inv = lax.rsqrt(jnp.sum(square, axis=-1, keepdims=True) / 2048.0 + EPS)
         for g in range(8):
-            xq[g] = (recv1[g, mine, :].astype(F32) * inv * gains[g : g + 1, :]).astype(BF)
+            xq[g, 0:n_rows, :] = (recv1[g, mine, :].astype(F32) * inv * gains[g : g + 1, :]).astype(BF)
 
         def rows_of(ref, g, cols):
             return jnp.concatenate([ref[n * 128 + g * 16 : n * 128 + g * 16 + 16, cols] for n in range(16)], axis=0)
 
         for n in range(2):
             cols = slice(n * 256, (n + 1) * 256)
-            gate = jnp.zeros((128, 256), F32)
-            up = jnp.zeros((128, 256), F32)
+            gate = jnp.zeros((n_rows, 256), F32)
+            up = jnp.zeros((n_rows, 256), F32)
             for g in range(8):
-                gate = gate + jnp.dot(xq[g], rows_of(egv, g, cols), preferred_element_type=F32)
-                up = up + jnp.dot(xq[g], rows_of(euv, g, cols), preferred_element_type=F32)
+                gate = gate + jnp.dot(xq[g, 0:n_rows, :], rows_of(egv, g, cols), preferred_element_type=F32)
+                up = up + jnp.dot(xq[g, 0:n_rows, :], rows_of(euv, g, cols), preferred_element_type=F32)
             hid[mine, cols] = (jax.nn.silu(gate) * up).astype(BF)
         for n in range(8):
             cols = slice(n * 256, (n + 1) * 256)
             out = jnp.dot(hid[mine, :], edv[:, cols], preferred_element_type=F32).astype(BF)
-            send2[half * 64 : half * 64 + 64, :, cols] = out.reshape(64, 2, 256)
-
-    dispatch(0)
-    dispatch(1)
+            send2[first // 2 : (first + n_rows) // 2, :, cols] = out.reshape(n_rows // 2, 2, 256)
+
+    for n in range(len(MOVES)):
+        dispatch(n)
     recv1[seat, 0:16, :] = send1[me]
     for there, its_seat in others:
         pltpu.make_async_remote_copy(

time: 51.4 us -> 50.2 us (0.977)
  Pallas kernels: 50.7 us -> 49.4 us
    pallas_call x1, Pallas kernels: 48.2 us -> 47 us  [shards(): pl.pallas_call(kernel, out_shape=(pltpu.VMEM(tokens.shape, BF), pltpu.VME...]
where the time goes in v5:
time: 50.2 us; the launch traced here: 50.1 us
  Pallas kernels  49.4 us (98%)
  between operations  0.64 us (1%)
    pallas_call x1, Pallas kernels, shards(): pl.pallas_call(kernel, out_shape=(pltpu.VMEM(tokens.shape, BF), pltpu.VME...  47 us
    pallas_call x1, Pallas kernels, shards(): pl.pallas_call(hand_over, out_shape=(jax.ShapeDtypeStruct(tokens.shape, B...  2.46 us

profile of v5, /device:TPU:1, one launch (start us, length us, event | category | flops | bytes accessed | tf_op | source)
XLA Modules:
  0.0 50.1 jit_solution(14285012151022869288)
XLA Ops:
  0.6 47.0 %layer.1 = (bf16[20,2048]{1,0:T(8,128)(2,1)S(1)}, f32[20,8,64,128]{3,2,1,0:T(8,128)S(1)}) custom-call(bf16[20,2048]{1,0:T(8,128)(2,1)} %tokens_h.1, s32[1,20]{1,0:T(1,128)} %bitcast.13, f32[1,2048]{1,0:T(1,128)} %bitcast.8, f32[1,1024]{1,0:T(1,128)} %bitcast.10, f32[1,2048]{1,0:T(1,128)} %bitcast.9, s32[6,20]{1,0:T(8,128)} %bitcast.11, f32[6,20]{1,0:T(8,128)} %bitcast.12, ...), custom_call_target="tpu_custom_call" | custom-call | tf_op jit(solution)/shard_map/layer/pallas_call | solution.py:441
  47.6 2.5 %hand_over.1 = (bf16[20,2048]{1,0:T(8,128)(2,1)}, f32[20,8,64,128]{3,2,1,0:T(8,128)}) custom-call(bf16[20,2048]{1,0:T(8,128)(2,1)S(1)} %get-tuple-element.4.result, f32[20,8,64,128]{3,2,1,0:T(8,128)S(1)} %get-tuple-element.5.new_state), custom_call_target="tpu_custom_call" | custom-call | tf_op jit(solution)/shard_map/hand_over/pallas_call | solution.py:469

commit v6 on v5

--- a/solution.py
+++ b/solution.py
@@ -26,7 +26,7 @@
 MOVES = [
     sorted(
         [(l, *LINES[l], x, c) for l in range(a, b) for x in range(4) for c in range(2) if LINES[l] + (x, c) != (0,) * 4],
-        key=lambda d: (-hops(d[1:]), d[3], -d[0], d[4]),
+        key=lambda d: (-hops(d[1:]), d[4], d[3], d[0]),
     )
     for a, b in zip(BOUNDS[:-1], BOUNDS[1:])
 ]
@@ -269,15 +269,6 @@
             send_sem=ps.at[2], recv_sem=pr.at[6], device_id=(there,), device_id_type=MESH,
         ).start()
     tok_in[seat] = tok_out[seat]
-    for n in (1, 2, 0):
-        its_seat = mates[n][1]
-        block = mix.at[0, pl.ds(0, 24)]
-        pltpu.make_async_copy(block, block, pr.at[2 + n]).wait()
-        block = mix.at[its_seat, pl.ds(0, 24)]
-        pltpu.make_async_remote_copy(
-            src_ref=block, dst_ref=block, send_sem=ps.at[0], recv_sem=pr.at[0],
-            device_id=(mates[3][0],), device_id_type=MESH,
-        ).start()
     routed = plan.at[pl.ds(0, 7)]
     pltpu.make_async_copy(routed, routed, pr.at[7]).wait()
     ids = jnp.concatenate([plan[g, :, 0:32] for g in range(8)], axis=1)
@@ -294,6 +285,15 @@
             member = jnp.where(shifted_ids[k : k + 1, :] == expert_f, mine_f, member)
         place = jnp.dot(member.astype(BF), earlier, preferred_element_type=F32)
         dall[b * 256 : (b + 1) * 256, :] = jnp.where(place == slot_f, member, 0.0).astype(BF)
+    for n in (1, 2, 0):
+        its_seat = mates[n][1]
+        block = mix.at[0, pl.ds(0, 24)]
+        pltpu.make_async_copy(block, block, pr.at[2 + n]).wait()
+        block = mix.at[its_seat, pl.ds(0, 24)]
+        pltpu.make_async_remote_copy(
+            src_ref=block, dst_ref=block, send_sem=ps.at[0], recv_sem=pr.at[0],
+            device_id=(mates[3][0],), device_id_type=MESH,
+        ).start()
     gathered(12, 2)
     gathered(12, 3)
     block = mix.at[0, pl.ds(0, 24)]

time: 50.2 us -> 50.3 us (level)
  no operation moved by 1% of the time
where the time goes in v6:
time: 50.3 us; the launch traced here: 50.2 us
  Pallas kernels  49.6 us (99%)
  between operations  0.64 us (1%)
    pallas_call x1, Pallas kernels, shards(): pl.pallas_call(kernel, out_shape=(pltpu.VMEM(tokens.shape, BF), pltpu.VME...  47.1 us
    pallas_call x1, Pallas kernels, shards(): pl.pallas_call(hand_over, out_shape=(jax.ShapeDtypeStruct(tokens.shape, B...  2.46 us

profile of v6, /device:TPU:1, one launch (start us, length us, event | category | flops | bytes accessed | tf_op | source)
XLA Modules:
  0.0 50.2 jit_solution(1722694770380431674)
XLA Ops:
  0.6 47.1 %layer.1 = (bf16[20,2048]{1,0:T(8,128)(2,1)S(1)}, f32[20,8,64,128]{3,2,1,0:T(8,128)S(1)}) custom-call(bf16[20,2048]{1,0:T(8,128)(2,1)} %tokens_h.1, s32[1,20]{1,0:T(1,128)} %bitcast.13, f32[1,2048]{1,0:T(1,128)} %bitcast.8, f32[1,1024]{1,0:T(1,128)} %bitcast.10, f32[1,2048]{1,0:T(1,128)} %bitcast.9, s32[6,20]{1,0:T(8,128)} %bitcast.11, f32[6,20]{1,0:T(8,128)} %bitcast.12, ...), custom_call_target="tpu_custom_call" | custom-call | tf_op jit(solution)/shard_map/layer/pallas_call | solution.py:441
  47.8 2.5 %hand_over.1 = (bf16[20,2048]{1,0:T(8,128)(2,1)}, f32[20,8,64,128]{3,2,1,0:T(8,128)}) custom-call(bf16[20,2048]{1,0:T(8,128)(2,1)S(1)} %get-tuple-element.4.result, f32[20,8,64,128]{3,2,1,0:T(8,128)S(1)} %get-tuple-element.5.new_state), custom_call_target="tpu_custom_call" | custom-call | tf_op jit(solution)/shard_map/hand_over/pallas_call | solution.py:469
